TPU v7x, 32 devices: a whole 2x2x4 slice. The times are simulated.
32 devices in a mesh: sp: 16 (over z, y, x), tp: 2 (over core).
Axes of the slice: x: 2, y: 2, z: 4, core: 2. Of those that a mesh axis runs over, the one named last changes fastest.
Arguments:
- residual: bfloat16 [4096, 2048], P(('sp', 'tp')), may hold values from -6 to 6
- pool_input: bfloat16 [4096, 1024], P('sp', 'tp'), may hold values from -6 to 6
- group_maps: bfloat16 [8, 128, 128], replicated, may hold values from -0.5 to 0.5
- pool_scale: float32 [1024], replicated, may hold values from 0.1 to 1.9
- out_proj: bfloat16 [1024, 2048], replicated, may hold values from -0.1875 to 0.1875
- norm_gain: float32 [2048], replicated, may hold values from 0.1 to 1.9
- shared_gate: bfloat16 [2048, 512], replicated, may hold values from -0.125 to 0.125
- shared_up: bfloat16 [2048, 512], replicated, may hold values from -0.125 to 0.125
- shared_down: bfloat16 [512, 2048], replicated, may hold values from -0.25 to 0.25
- expert_gate: bfloat16 [32, 2048, 512], P(('sp', 'tp')), may hold values from -0.125 to 0.125
- expert_up: bfloat16 [32, 2048, 512], P(('sp', 'tp')), may hold values from -0.125 to 0.125
- expert_down: bfloat16 [32, 512, 2048], P(('sp', 'tp')), may hold values from -0.25 to 0.25
- expert_ids: int32 [4096, 4], P(('sp', 'tp')), may hold values from 0 to 31, all different within a row; in each aligned block of 128 rows (0 to 127, 128 to 255, ...) at most 24 rows name the same one
- route_score: float32 [4096, 4], P(('sp', 'tp')), may hold values from 0.05 to 1
Outputs:
- output: bfloat16 [4096, 2048], P(('sp', 'tp'))
Inputs may be any that keep to these rules, and one draw needn't show every extreme that they name: `expert_ids`: each row names 4 different experts; among the 128 rows of one device no expert is named more than 24 times, and in some devices' rows one expert is named exactly 24 times.
All inputs are finite; a program needn't handle non-finite values.
Results may differ from a plain program's by a relative error of at most 0.015.
Values may be sent and summed in bfloat16 or wider, within the bound.
A program may use at most 128 MiB of HBM per device.

v0:
```python
import functools
import math

import jax
import jax.numpy as jnp
from jax import lax
from jax.experimental import pallas as pl
from jax.experimental.pallas import tpu as pltpu
from jax.sharding import PartitionSpec as P

windows = (2, 4, 8, 16)
epsilon = 1e-06
routed_scale = 2.5


def from_behind(shard, axis, by):
    peers = lax.axis_size(axis)
    pairs = [(i, i + by) for i in range(peers) if 0 <= i + by < peers]
    return lax.ppermute(shard, axis, pairs)


def layer_count(size_sp):
    return max(d for d in range(1, math.isqrt(size_sp) + 1) if size_sp % d == 0)


def moe_kernel(
    layers,
    peers,
    cores,
    cap,
    top,
    normed_ref,
    settled_ref,
    meta_ref,
    sg_hbm,
    su_hbm,
    sd_hbm,
    eg_hbm,
    eu_hbm,
    ed_hbm,
    out_ref,
    gathered,
    metas,
    packed,
    arrived,
    results,
    back,
    part,
    landed,
    acc,
    sg,
    su,
    sd,
    eg,
    eu,
    ed,
    w_sem,
    own_sem,
    z_send,
    z_recv,
    m_send,
    m_recv,
    a_send,
    a_recv,
    b_send,
    b_recv,
    c_send,
    c_recv,
):
    per_layer = peers // cores
    sp = lax.axis_index("sp")
    core = lax.axis_index("tp")
    z = sp // per_layer
    q = sp % per_layer
    me = q * cores + core
    tokens, width = normed_ref.shape
    slots = peers * cap
    step_cols = min(width, 512)

    def in_column(s):
        return (s * per_layer + q, core)

    def in_layer(p):
        return (z * per_layer + p // cores, p % cores)

    def remote(src, dst, send, recv, to):
        return pltpu.make_async_remote_copy(
            src_ref=src,
            dst_ref=dst,
            send_sem=send,
            recv_sem=recv,
            device_id=to,
            device_id_type=pl.DeviceIdType.MESH,
        )

    loads = [
        pltpu.make_async_copy(a, b, w_sem.at[i])
        for i, (a, b) in enumerate(
            (
                (sg_hbm, sg),
                (su_hbm, su),
                (sd_hbm, sd),
                (eg_hbm.at[0], eg),
                (eu_hbm.at[0], eu),
                (ed_hbm.at[0], ed),
            )
        )
    ]
    own_rows = pltpu.make_async_copy(normed_ref, gathered.at[z], own_sem.at[0])
    own_meta = pltpu.make_async_copy(meta_ref, metas.at[z], own_sem.at[1])
    own_rows.start()
    own_meta.start()
    for load in loads:
        load.start()

    barrier = pltpu.get_barrier_semaphore()
    for o in range(1, layers):
        pl.semaphore_signal(
            barrier, inc=1, device_id=in_column((z + o) % layers),
            device_id_type=pl.DeviceIdType.MESH,
        )
    for o in range(1, peers):
        pl.semaphore_signal(
            barrier, inc=1, device_id=in_layer((me + o) % peers),
            device_id_type=pl.DeviceIdType.MESH,
        )
    pl.semaphore_wait(barrier, layers - 1 + peers - 1)
    own_rows.wait()
    own_meta.wait()

    def meta_copy(target, source):
        return remote(
            metas.at[source], metas.at[source], m_send.at[target], m_recv.at[source],
            in_column(target),
        )

    for o in range(1, layers):
        meta_copy((z + o) % layers, z).start()

    def chunk_copy(s, side):
        to = z + 1 if side == 0 else z - 1
        to = jnp.clip(to, 0, layers - 1)
        return remote(
            gathered.at[s], gathered.at[s], z_send.at[side, s], z_recv.at[s], in_column(to)
        )

    def goes_up(s):
        return jnp.logical_and(s <= z, z < layers - 1)

    def goes_down(s):
        return jnp.logical_and(s >= z, z > 0)

    def pack_copy(s, p, source):
        return remote(
            packed.at[s, p], arrived.at[s, source], a_send.at[s, p], a_recv.at[s, source],
            in_layer(p),
        )

    def back_copy(s, p, source):
        return remote(
            results.at[s, p], back.at[s, source], b_send.at[s, p], b_recv.at[s, source],
            in_layer(p),
        )

    def part_copy(s, source):
        return remote(
            part.at[s], landed.at[source], c_send.at[s], c_recv.at[source], in_column(s)
        )

    def own_pack(s):
        return pltpu.make_async_copy(packed.at[s, me], arrived.at[s, me], a_recv.at[s, me])

    def own_back(s):
        return pltpu.make_async_copy(results.at[s, me], back.at[s, me], b_recv.at[s, me])

    far_first = sorted(range(1, peers), key=lambda o: (o % cores, -o % 3, o))
    near = jnp.minimum(z, layers - 1 - z)

    def chunk_at(i):
        both = (i + 1) // 2
        two_sided = jnp.where(i % 2 == 1, z - both, z + both)
        one_sided = jnp.where(2 * z <= layers - 1, z + (i - near), z - (i - near))
        return jnp.where(i <= 2 * near, two_sided, one_sided)

    def slot_table(s, value):
        ids = lax.broadcasted_iota(jnp.int32, (slots, tokens), 0).astype(jnp.float32)
        ids = ids + (z * slots).astype(jnp.float32)
        table = jnp.zeros((slots, tokens), jnp.float32)
        rows = metas[s]
        for k in range(top):
            hit = ids == rows[k : k + 1]
            table = table + jnp.where(hit, rows[top + k : top + k + 1] if value else 1.0, 0.0)
        return table

    def dispatch(i):
        s = chunk_at(i)

        @pl.when(i > 0)
        def _():
            chunk_copy(s, 0).wait_recv()

        @pl.when(goes_up(s))
        def _():
            chunk_copy(s, 0).start()

        @pl.when(goes_down(s))
        def _():
            chunk_copy(s, 1).start()

        @pl.when(i > 0)
        def _():
            meta_copy(z, s).wait_recv()

        table = slot_table(s, False).astype(jnp.bfloat16)
        for col in range(0, width, step_cols):
            got = jnp.dot(
                table, gathered[s, :, col : col + step_cols], preferred_element_type=jnp.float32
            )
            packed[s, :, :, col : col + step_cols] = (
                got.astype(jnp.bfloat16).reshape(peers, cap, step_cols)
            )
        for o in far_first:
            pack_copy(s, (me + o) % peers, me).start()
        own_pack(s).start()

    def mlp(rows, w_gate, w_up):
        gate = jnp.dot(rows, w_gate[...], preferred_element_type=jnp.float32)
        up = jnp.dot(rows, w_up[...], preferred_element_type=jnp.float32)
        return (gate / (1.0 + jnp.exp(-gate)) * up).astype(jnp.bfloat16)

    def expert(i):
        s = chunk_at(i)
        for o in range(1, peers):
            p = (me + o) % peers
            pack_copy(s, p, p).wait_recv()
        own_pack(s).wait()
        hidden = mlp(arrived[s].reshape(slots, width), eg, eu)
        for col in range(0, width, step_cols):
            got = jnp.dot(hidden, ed[:, col : col + step_cols], preferred_element_type=jnp.float32)
            results[s, :, :, col : col + step_cols] = (
                got.astype(jnp.bfloat16).reshape(peers, cap, step_cols)
            )
        for o in far_first:
            back_copy(s, (me + o) % peers, me).start()
        own_back(s).start()

    def combine(i):
        s = chunk_at(i)
        for o in range(1, peers):
            p = (me + o) % peers
            back_copy(s, p, p).wait_recv()
        own_back(s).wait()
        table = slot_table(s, True)
        high = table.astype(jnp.bfloat16)
        low = (table - high.astype(jnp.float32)).astype(jnp.bfloat16)
        dims = (((0,), (0,)), ((), ()))
        for col in range(0, width, step_cols):
            rows = back[s, :, :, col : col + step_cols].reshape(slots, step_cols)
            got = lax.dot_general(high, rows, dims, preferred_element_type=jnp.float32)
            got = got + lax.dot_general(low, rows, dims, preferred_element_type=jnp.float32)

            @pl.when(i == 0)
            def _():
                acc[:, col : col + step_cols] = acc[:, col : col + step_cols] + got

            @pl.when(i > 0)
            def _():
                part[s, :, col : col + step_cols] = got.astype(jnp.bfloat16)

        @pl.when(i > 0)
        def _():
            part_copy(s, z).start()

    def shared():
        for load in loads[:3]:
            load.wait()
        hidden = mlp(normed_ref[...], sg, su)
        for col in range(0, width, step_cols):
            got = jnp.dot(hidden, sd[:, col : col + step_cols], preferred_element_type=jnp.float32)
            acc[:, col : col + step_cols] = got + settled_ref[:, col : col + step_cols].astype(
                jnp.float32
            )

    at_end = near == 0

    def step(i, carry):
        later = jnp.logical_and(i >= 3, at_end)

        @pl.when(later)
        def _():
            combine(i - 2)

        @pl.when(i < layers)
        def _():
            dispatch(i)

        @pl.when(i >= 2)
        def _():
            expert(i - 1)

        @pl.when(jnp.logical_and(i >= 3, jnp.logical_not(at_end)))
        def _():
            combine(i - 2)

        return carry

    def last(j, carry):
        combine((layers - 1) * (1 - j))
        return carry

    dispatch(jnp.int32(0))
    shared()
    for load in loads[3:]:
        load.wait()
    lax.fori_loop(1, layers + 1, step, 0)
    expert(jnp.int32(0))
    lax.fori_loop(0, 2, last, 0)

    def drain(s, carry):
        @pl.when(goes_up(s))
        def _():
            chunk_copy(s, 0).wait_send()

        @pl.when(goes_down(s))
        def _():
            chunk_copy(s, 1).wait_send()

        for o in range(1, peers):
            p = (me + o) % peers
            pack_copy(s, p, me).wait_send()
            back_copy(s, p, me).wait_send()
        return carry

    lax.fori_loop(0, layers, drain, 0)
    for o in range(1, layers):
        s = (z + o) % layers
        meta_copy(s, z).wait_send()
        part_copy(s, z).wait_send()
        part_copy(s, s).wait_recv()
    for col in range(0, width, step_cols):
        total = acc[:, col : col + step_cols]
        for o in range(1, layers):
            s = (z + o) % layers
            total = total + landed[s, :, col : col + step_cols].astype(jnp.float32)
        out_ref[:, col : col + step_cols] = total.astype(jnp.bfloat16)


def on_device(
    residual,
    pool_input,
    group_maps,
    pool_scale,
    out_proj,
    norm_gain,
    shared_gate,
    shared_up,
    shared_down,
    expert_gate,
    expert_up,
    expert_down,
    expert_ids,
    route_score,
):
    row_count, channels = pool_input.shape
    group_width = group_maps.shape[1]
    groups_here = channels // group_width
    halo_reach = max(windows) - 1
    before = from_behind(pool_input[row_count - halo_reach :], "sp", 1)
    extended = (
        jnp.concatenate([before, pool_input], axis=0)
        .astype(jnp.float32)
        .reshape(row_count + halo_reach, groups_here, group_width)
    )
    places = lax.axis_index("sp") * row_count + jnp.arange(row_count, dtype=jnp.int32)
    pooled = []
    for group_index in range(groups_here):
        running_sum = extended[:, group_index]
        window_span = 1
        while window_span < windows[group_index % 4]:
            running_sum = running_sum[window_span:] + running_sum[:-window_span]
            window_span = window_span * 2
        divisor = jnp.minimum(places + 1, window_span).astype(jnp.float32)[:, None]
        pooled.append(running_sum[running_sum.shape[0] - row_count :] / divisor)
    pooled = jnp.stack(pooled, axis=1)
    contrast = (pooled - extended[halo_reach:]).astype(jnp.bfloat16)
    first_group = lax.axis_index("tp") * groups_here
    maps_here = lax.dynamic_slice_in_dim(group_maps, first_group, groups_here, 0)
    mapped = jnp.einsum("sgc,gcd->sgd", contrast, maps_here, preferred_element_type=jnp.float32)
    scale_here = lax.dynamic_slice_in_dim(pool_scale, first_group * group_width, channels, 0)
    mixed_rows = (mapped.reshape(row_count, channels) * scale_here).astype(jnp.bfloat16)
    model_width = out_proj.shape[1]
    swapped = lax.all_to_all(mixed_rows, "tp", split_axis=0, concat_axis=1, tiled=True)
    projected = jnp.dot(swapped, out_proj, preferred_element_type=jnp.float32)
    settled = (residual.astype(jnp.float32) + projected).astype(jnp.bfloat16)
    settled_wide = settled.astype(jnp.float32)
    inverse_rms = lax.rsqrt(jnp.mean(settled_wide * settled_wide, axis=-1, keepdims=True) + epsilon)
    normed = (settled_wide * inverse_rms * norm_gain).astype(jnp.bfloat16)
    tokens_here, top_count = expert_ids.shape
    size_sp = lax.axis_size("sp")
    size_tp = lax.axis_size("tp")
    experts = size_sp * size_tp
    capacity = 3 * tokens_here * top_count // (2 * experts)
    cap = -(-capacity // 8) * 8
    layers = layer_count(size_sp)
    peers = experts // layers
    assigned = tokens_here * top_count
    flat_ids = expert_ids.reshape(assigned)
    onehot = (flat_ids[:, None] == jnp.arange(experts, dtype=jnp.int32)[None, :]).astype(
        jnp.bfloat16
    )
    earlier = (jnp.arange(assigned)[None, :] < jnp.arange(assigned)[:, None]).astype(jnp.bfloat16)
    before_counts = jnp.dot(earlier, onehot, preferred_element_type=jnp.float32)
    position = jnp.sum(before_counts * onehot, axis=1)
    slot = (flat_ids.astype(jnp.float32) * cap + position).reshape(tokens_here, top_count)
    weights = route_score / jnp.sum(route_score, axis=-1, keepdims=True) * routed_scale
    meta = jnp.concatenate([slot, weights], axis=1).T
    hidden_width = shared_gate.shape[1]
    expert_width = expert_gate.shape[2]
    any_spec = pl.BlockSpec(memory_space=pl.ANY)
    vmem_spec = pl.BlockSpec(memory_space=pltpu.VMEM)
    bf16, f32 = jnp.bfloat16, jnp.float32
    dma = pltpu.SemaphoreType.DMA
    routed = (layers, peers, cap, model_width)
    chunks = (layers, tokens_here, model_width)
    return pl.pallas_call(
        functools.partial(moe_kernel, layers, peers, size_tp, cap, top_count),
        out_shape=jax.ShapeDtypeStruct((tokens_here, model_width), bf16),
        in_specs=[vmem_spec] * 3 + [any_spec] * 6,
        out_specs=vmem_spec,
        scratch_shapes=[
            pltpu.VMEM(chunks, bf16),
            pltpu.VMEM((layers, 2 * top_count, tokens_here), f32),
            pltpu.VMEM(routed, bf16),
            pltpu.VMEM(routed, bf16),
            pltpu.VMEM(routed, bf16),
            pltpu.VMEM(routed, bf16),
            pltpu.VMEM(chunks, bf16),
            pltpu.VMEM(chunks, bf16),
            pltpu.VMEM((tokens_here, model_width), f32),
            pltpu.VMEM((model_width, hidden_width), bf16),
            pltpu.VMEM((model_width, hidden_width), bf16),
            pltpu.VMEM((hidden_width, model_width), bf16),
            pltpu.VMEM((model_width, expert_width), bf16),
            pltpu.VMEM((model_width, expert_width), bf16),
            pltpu.VMEM((expert_width, model_width), bf16),
            dma((6,)),
            dma((2,)),
            dma((2, layers)),
            dma((layers,)),
            dma((layers,)),
            dma((layers,)),
            dma((layers, peers)),
            dma((layers, peers)),
            dma((layers, peers)),
            dma((layers, peers)),
            dma((layers,)),
            dma((layers,)),
        ],
        compiler_params=pltpu.CompilerParams(
            collective_id=0, has_side_effects=True, vmem_limit_bytes=44 * 1024 * 1024
        ),
    )(
        normed,
        settled,
        meta,
        shared_gate,
        shared_up,
        shared_down,
        expert_gate,
        expert_up,
        expert_down,
    )


def solution(mesh):
    in_specs = (
        P(("sp", "tp"), None),
        P("sp", "tp"),
        P(),
        P(),
        P(),
        P(),
        P(),
        P(),
        P(),
        P(("sp", "tp"), None, None),
        P(("sp", "tp"), None, None),
        P(("sp", "tp"), None, None),
        P(("sp", "tp"), None),
        P(("sp", "tp"), None),
    )
    out_specs = P(("sp", "tp"), None)
    return jax.shard_map(
        on_device, mesh=mesh, in_specs=in_specs, out_specs=out_specs, check_vma=False
    )
```

profile of v0, /device:TPU:29, one launch (start us, length us, event | category | flops | bytes accessed | tf_op | source)
XLA Modules:
  0.0 129.1 jit_solution(8189540856810040470)
XLA Ops:
  0.0 0.0 copy-start
  0.0 0.8 slice.118
  0.8 3.1 %collective-permute-start = (bf16[15,512]{1,0:T(8,128)(2,1)S(1)}, bf16[15,512]{1,0:T(8,128)(2,1)S(1)}, u32[]{:S(2)}, u32[]{:S(2)}) collective-permute-start(bf16[15,512]{1,0:T(8,128)(2,1)S(1)} %slice.118), channel_id=1, source_target_pairs={{0,2},{2,4},{4,6},{6,8},{8,10},{10,12},{12,14},{14,16},{16,18},{18... | collective-permute-start | bytes 46088 | tf_op jit(solution)/shard_map/ppermute | solution.py:19
  3.9 1.0 copy_bitcast_fusion
  4.9 0.8 copy.24
  5.7 0.1 eq.15
  5.8 0.3 fusion.1
  6.1 0.1 reduce_sum.31
  6.2 0.1 copy.25
  6.3 0.7 reduce_sum.32
  7.0 0.7 divide_multiply_fusion
  7.7 0.8 dynamic_slice.7
  8.5 0.0 collective-permute-done
  8.5 0.1 maximum_convert_fusion
  8.6 0.1 fusion.25
  8.7 0.0 copy-start.5
  8.8 0.1 fusion.10
  8.9 0.1 fusion.19
  9.0 0.1 fusion.13
  9.1 0.1 fusion.16
  9.3 0.0 copy-done
  9.3 0.3 copy-done.5
  9.6 0.3 convolution_bitcast_fusion
  9.9 0.0 copy-start.4
  9.9 0.3 reshape.84
  10.2 0.1 fusion.6
  10.3 0.0 copy-start.6
  10.3 4.7 %all_to_all.16 = bf16[2,128,512]{1,2,0:T(8,128)(2,1)S(1)} all-to-all(bf16[2,128,512]{1,2,0:T(8,128)(2,1)S(1)} %fusion.6), channel_id=1, replica_groups=mesh['sp'=16,'tp'=2] {'tp'}, dimensions={0} | all-to-all | bytes 524288 | tf_op jit(solution)/shard_map/all_to_all | solution.py:392
  15.0 0.0 copy-start.1
  15.0 0.0 copy-start.2
  15.0 0.0 copy-start.3
  15.0 3.3 %fusion.2 = (f32[128]{0:T(128)S(1)}, bf16[128,2048]{1,0:T(8,128)(2,1)S(1)}) fusion(bf16[128,1024]{0,1:T(8,128)(2,1)S(1)} %bitcast.54, bf16[1024,2048]{1,0:T(8,128)(2,1)} %param.18, bf16[128,2048]{1,0:T(8,128)(2,1)} %param.14), kind=kOutput, calls=%fused_computation.7 | convolution fusion | flops 538443648 | bytes 5505536 | tf_op jit(solution)/shard_map/dot_general | solution.py:393
  18.3 0.0 copy-done.6
  18.3 0.2 fusion.4.normed_ref
  18.5 0.0 copy-done.4
  18.5 0.0 copy-done.1
  18.5 0.1 copy-done.2
  18.6 0.6 copy-done.3
  19.3 109.0 %shard_map.136 = bf16[128,2048]{1,0:T(8,128)(2,1)S(1)} custom-call(bf16[128,2048]{1,0:T(8,128)(2,1)S(1)} %fusion.4.normed_ref, bf16[128,2048]{1,0:T(8,128)(2,1)S(1)} %get-tuple-element.15.settled_ref, f32[8,128]{1,0:T(8,128)S(1)} %maximum_bitcast_fusion.meta_ref, bf16[2048,512]{1,0:T(8,128)(2,1)S(1)} %copy-done.1, bf16[2048,512]{1,0:T(8,128)(2,1)S(1)} %copy-done.2, ...), custom_call_target="tpu_custom_call" | custom-call | tf_op jit(solution)/shard_map/pallas_call | solution.py:425
  128.3 0.8 copy.36
  (10 shorter events, 0.1 us)
Async XLA Ops:
  0.0 9.3 %copy-start = (bf16[8,128,128]{2,1,0:T(8,128)(2,1)S(1)}, bf16[8,128,128]{2,1,0:T(8,128)(2,1)}, u32[]{:S(2)}) copy-start(bf16[8,128,128]{2,1,0:T(8,128)(2,1)} %param.16) | copy-start | bytes 786436
  0.8 7.7 %collective-permute-start = (bf16[15,512]{1,0:T(8,128)(2,1)S(1)}, bf16[15,512]{1,0:T(8,128)(2,1)S(1)}, u32[]{:S(2)}, u32[]{:S(2)}) collective-permute-start(bf16[15,512]{1,0:T(8,128)(2,1)S(1)} %slice.118), channel_id=1, source_target_pairs={{0,2},{2,4},{4,6},{6,8},{8,10},{10,12},{12,14},{14,16},{16,18},{18... | collective-permute-start | bytes 46088 | tf_op jit(solution)/shard_map/ppermute | solution.py:19
  8.7 1.0 copy-start.5
  9.9 8.6 %copy-start.4 = (bf16[1,2048,512]{2,1,0:T(8,128)(2,1)S(1)}, bf16[1,2048,512]{2,1,0:T(8,128)(2,1)}, u32[]{:S(2)}) copy-start(bf16[1,2048,512]{2,1,0:T(8,128)(2,1)} %eg_hbm.1) | copy-start | bytes 6291460
  10.3 8.0 %copy-start.6 = (f32[2048]{0:T(1024)S(1)}, f32[2048]{0:T(1024)}, u32[]{:S(2)}) copy-start(f32[2048]{0:T(1024)} %param.19) | copy-start | bytes 24580
  15.0 3.5 %copy-start.1 = (bf16[2048,512]{1,0:T(8,128)(2,1)S(1)}, bf16[2048,512]{1,0:T(8,128)(2,1)}, u32[]{:S(2)}) copy-start(bf16[2048,512]{1,0:T(8,128)(2,1)} %sg_hbm.1) | copy-start | bytes 6291460
  15.0 3.6 %copy-start.2 = (bf16[2048,512]{1,0:T(8,128)(2,1)S(1)}, bf16[2048,512]{1,0:T(8,128)(2,1)}, u32[]{:S(2)}) copy-start(bf16[2048,512]{1,0:T(8,128)(2,1)} %su_hbm.1) | copy-start | bytes 6291460
  15.0 4.3 %copy-start.3 = (bf16[512,2048]{1,0:T(8,128)(2,1)S(1)}, bf16[512,2048]{1,0:T(8,128)(2,1)}, u32[]{:S(2)}) copy-start(bf16[512,2048]{1,0:T(8,128)(2,1)} %sd_hbm.1) | copy-start | bytes 6291460
where the time goes:
time: 130 us; the launch traced here: 129 us
  Pallas kernels  109 us (84%)
  local copies, waits for them, and re-layouts  5.83 us (4%)
  blocking collectives  4.67 us (4%)
  matrix products  3.85 us (3%)
  starting transfers between devices  3.11 us (2%)
  other arithmetic  2.39 us (2%)
    pallas_call x1, Pallas kernels, on_device(): pl.pallas_call(functools.partial(moe_kernel, layers, peers, size_tp, cap,...  109 us
    all_to_all x1, blocking collectives, on_device(): lax.all_to_all(mixed_rows, 'tp', split_axis=0, concat_axis=1, tiled=True)  4.67 us
    dot_general x1, matrix products, on_device(): projected = jnp.dot(swapped, out_proj, preferred_element_type=jnp.float32)  3.29 us
    ppermute x1, starting transfers between devices, from_behind(): return lax.ppermute(shard, axis, pairs)  3.11 us
    unnamed x16, local copies, waits for them, and re-layouts  2.7 us
  transfers between devices with their start and end apart: 1, of which 0 were waited for; matrix products, arithmetic and copies ran while one was open for 4% of the time, Pallas kernels for 0%

commit v1 on v0

v1 whole, which is shorter than its diff:
```python
import functools
import math

import jax
import jax.numpy as jnp
from jax import lax
from jax.experimental import pallas as pl
from jax.experimental.pallas import tpu as pltpu
from jax.sharding import PartitionSpec as P

windows = (2, 4, 8, 16)
epsilon = 1e-06
routed_scale = 2.5
halo_rows = 16
NOP, ARRIVE, EXPERT, COMBINE, SHARED = range(5)


def layer_count(size_sp):
    return max(d for d in range(1, math.isqrt(size_sp) + 1) if size_sp % d == 0)


END = (
    "a0", "a1", "s0", "a2", "a3", "a4", "a5", "a6", "e2",
    "a7", "c2", "e3", "e1", "c3", "c1", "e0", "c0",
)
MIDDLE = (
    "a0", "a1", "s0", "a2", "a3", "a4", "a5", "e3",
    "e2", "e1", "e0", "c2", "c3", "c0", "c1",
)


def steps_of(z, layers):
    last = layers - 1
    if layers == 4:
        kinds = {"a": ARRIVE, "e": EXPERT, "c": COMBINE, "s": SHARED}
        steps = []
        for word in END if z in (0, last) else MIDDLE:
            value = int(word[1:])
            if word[0] in "ec" and 2 * z > last:
                value = last - value
            steps.append((kinds[word[0]], value))
        return steps
    at = lambda r: [s for s in (z - r, z + r) if 0 <= s < layers]
    reach = max(z, last - z)
    steps = [(ARRIVE, 0), (ARRIVE, 1), (SHARED, 0)]
    for r in range(1, reach + 1):
        steps += [(ARRIVE, 2 * r), (ARRIVE, 2 * r + 1)]
        steps += [(EXPERT, s) for s in sorted(set(at(r - 1)))]
    steps += [(EXPERT, s) for s in at(reach)]
    for r in range(reach, 0, -1):
        steps += [(COMBINE, s) for s in at(r)]
    return steps + [(COMBINE, z)]


def layer_kernel(
    layers,
    peers,
    cores,
    cap,
    residual_hbm,
    pool_hbm,
    maps_hbm,
    scale_hbm,
    proj_hbm,
    gain_hbm,
    sg_hbm,
    su_hbm,
    sd_hbm,
    eg_hbm,
    eu_hbm,
    ed_hbm,
    ids_hbm,
    score_hbm,
    out_ref,
    residual,
    pool,
    halo,
    maps,
    scale,
    gain,
    ids,
    score,
    mixed,
    swapped,
    proj,
    gathered,
    metas,
    tables,
    weigh,
    packed,
    arrived,
    results,
    back,
    part,
    landed,
    acc,
    sg,
    su,
    sd,
    eg,
    eu,
    ed,
    w_sem,
    h_sem,
    x_send,
    x_recv,
    z_send,
    z_recv,
    m_send,
    m_recv,
    a_send,
    a_recv,
    b_send,
    b_recv,
    c_send,
    c_recv,
):
    per_layer = peers // cores
    sp = lax.axis_index("sp")
    size_sp = layers * per_layer
    core = lax.axis_index("tp")
    z = sp // per_layer
    q = sp % per_layer
    me = q * cores + core
    blocks, tokens, cols = acc.shape
    width = blocks * cols
    slots = peers * cap
    top = ids.shape[1]
    rows, channels = pool.shape
    group_width = maps.shape[1]
    groups_here = channels // group_width
    f32, bf16 = jnp.float32, jnp.bfloat16

    def in_column(s):
        return (s * per_layer + q, core)

    def in_layer(p):
        return (z * per_layer + p // cores, p % cores)

    def remote(src, dst, send, recv, to):
        return pltpu.make_async_remote_copy(
            src_ref=src,
            dst_ref=dst,
            send_sem=send,
            recv_sem=recv,
            device_id=to,
            device_id_type=pl.DeviceIdType.MESH,
        )

    def tell(to):
        pl.semaphore_signal(
            pltpu.get_barrier_semaphore(), inc=1, device_id=to,
            device_id_type=pl.DeviceIdType.MESH,
        )

    first = pl.multiple_of(core * groups_here, groups_here)
    own_channels = pl.ds(pl.multiple_of(core * channels, channels), channels)
    pairs = (
        (pool_hbm, pool),
        (ids_hbm, ids),
        (score_hbm, score),
        (maps_hbm.at[pl.ds(first, groups_here)], maps),
        (scale_hbm.at[:, own_channels], scale),
        (proj_hbm, proj),
        (residual_hbm, residual),
        (gain_hbm, gain),
        (sg_hbm, sg),
        (su_hbm, su),
        (sd_hbm, sd),
        (eg_hbm.at[0], eg),
        (eu_hbm.at[0], eu),
        (ed_hbm.at[0], ed),
    )
    loads = [pltpu.make_async_copy(a, b, w_sem.at[i]) for i, (a, b) in enumerate(pairs)]
    for load in loads[:5]:
        load.start()
    for o in range(1, layers):
        tell(in_column((z + o) % layers))
    for o in range(1, peers):
        tell(in_layer((me + o) % peers))

    @pl.when(sp > 0)
    def _():
        tell((sp - 1, core))

    for load in loads[5:]:
        load.start()

    loads[1].wait()
    loads[2].wait()
    experts = layers * peers
    ids_now = ids[...]
    score_now = score[...]
    expert_at = lax.broadcasted_iota(jnp.int32, (tokens, experts), 1)
    named = [(ids_now[:, k : k + 1] == expert_at).astype(f32) for k in range(top)]
    named_any = functools.reduce(jnp.add, named).astype(bf16)
    earlier = (
        lax.broadcasted_iota(jnp.int32, (tokens, tokens), 1)
        < lax.broadcasted_iota(jnp.int32, (tokens, tokens), 0)
    ).astype(bf16)
    rank = jnp.dot(earlier, named_any, preferred_element_type=f32)
    shares = score_now / jnp.sum(score_now, axis=1, keepdims=True) * routed_scale
    lane = lax.broadcasted_iota(jnp.int32, (tokens, 128), 1)
    meta = jnp.zeros((tokens, 128), f32)
    for k in range(top):
        position = jnp.sum(rank * named[k], axis=1, keepdims=True)
        slot = ids_now[:, k : k + 1].astype(f32) * cap + position
        meta = jnp.where(lane == k, slot, meta)
        meta = jnp.where(lane == top + k, shares[:, k : k + 1], meta)
    metas[z] = jnp.transpose(meta)[: 2 * top]

    pl.semaphore_wait(
        pltpu.get_barrier_semaphore(),
        layers - 1 + peers - 1 + jnp.where(sp < size_sp - 1, 1, 0),
    )

    def halo_copy():
        return remote(
            pool.at[pl.ds(rows - halo_rows, halo_rows)], halo, h_sem.at[0], h_sem.at[1],
            (jnp.minimum(sp + 1, size_sp - 1), core),
        )

    loads[0].wait()

    @pl.when(sp < size_sp - 1)
    def _():
        halo_copy().start()

    def meta_copy(target, source):
        return remote(
            metas.at[source], metas.at[source], m_send.at[target], m_recv.at[source],
            in_column(target),
        )

    for o in range(1, layers):
        meta_copy((z + o) % layers, z).start()

    def chunk_copy(s, k, side):
        to = jnp.clip(jnp.where(side == 0, z + 1, z - 1), 0, layers - 1)
        return remote(
            gathered.at[s, k], gathered.at[s, k], z_send.at[side, s, k], z_recv.at[s, k],
            in_column(to),
        )

    def pack_copy(s, k, p, source):
        return remote(
            packed.at[s, k, p], arrived.at[s, k, source], a_send.at[s, k, p],
            a_recv.at[s, k, source], in_layer(p),
        )

    def back_copy(s, k, p, source):
        return remote(
            results.at[s, k, p], back.at[s, k, source], b_send.at[s, k, p],
            b_recv.at[s, k, source], in_layer(p),
        )

    def own_pack(s, k):
        return pltpu.make_async_copy(
            packed.at[s, k, me], arrived.at[s, k, me], a_recv.at[s, k, me]
        )

    def own_back(s, k):
        return pltpu.make_async_copy(
            results.at[s, k, me], back.at[s, k, me], b_recv.at[s, k, me]
        )

    def part_copy(s, k, side):
        to = jnp.clip(jnp.where(side == 0, z + 1, z - 1), 0, layers - 1)
        return remote(
            part.at[s, k], landed.at[side, s, k], c_send.at[s, k], c_recv.at[side, s, k],
            in_column(to),
        )

    far_first = sorted(range(1, peers), key=lambda o: (o % cores, -o % 3, o))

    @pl.when(sp == 0)
    def _():
        halo[...] = jnp.zeros(halo.shape, bf16)

    @pl.when(sp > 0)
    def _():
        halo_copy().wait_recv()

    loads[3].wait()
    loads[4].wait()
    half = rows // cores
    place = sp * rows + lax.broadcasted_iota(jnp.int32, (rows, group_width), 0)
    for g in range(groups_here):
        lanes = slice(g * group_width, (g + 1) * group_width)
        own = pool[:, lanes].astype(f32)
        total = jnp.concatenate([halo[:, lanes].astype(f32), own], axis=0)
        span = 1
        while span < windows[g % 4]:
            total = total + pltpu.roll(total, span, 0)
            span = span * 2
        divisor = jnp.minimum(place + 1, span).astype(f32)
        contrast = (total[halo_rows:] / divisor - own).astype(bf16)
        mapped = jnp.dot(contrast, maps[g], preferred_element_type=f32)
        mapped = (mapped * scale[:, lanes]).astype(bf16)
        for c in range(cores):
            mixed[c, :, lanes] = mapped[c * half : (c + 1) * half]

    def swap_copy(p, source):
        return remote(
            mixed.at[p], swapped.at[source], x_send.at[p], x_recv.at[source], (sp, p)
        )

    for o in range(1, cores):
        swap_copy((core + o) % cores, core).start()
    loads[5].wait()
    loads[6].wait()
    loads[7].wait()

    def channels_of(c):
        return pl.ds(pl.multiple_of(c * channels, channels), channels)

    for k in range(blocks):
        lanes = slice(k * cols, (k + 1) * cols)
        acc[k] = residual[:, lanes].astype(f32) + jnp.dot(
            mixed[core], proj[channels_of(core), lanes], preferred_element_type=f32
        )
    squares = jnp.zeros((tokens, 1), f32)
    for o in range(1, cores):
        p = (core + o) % cores
        swap_copy(p, p).wait_recv()
        for k in range(blocks):
            lanes = slice(k * cols, (k + 1) * cols)
            acc[k] = acc[k] + jnp.dot(
                swapped[p], proj[channels_of(p), lanes], preferred_element_type=f32
            )
    for k in range(blocks):
        settled = acc[k].astype(bf16).astype(f32)
        acc[k] = settled
        squares = squares + jnp.sum(settled * settled, axis=1, keepdims=True)
    inverse = lax.rsqrt(squares / width + epsilon)
    for k in range(blocks):
        gathered[z, k] = (acc[k] * inverse * gain[:, k * cols : (k + 1) * cols]).astype(bf16)

        @pl.when(z < layers - 1)
        def _():
            chunk_copy(z, k, 0).start()

        @pl.when(z > 0)
        def _():
            chunk_copy(z, k, 1).start()

    def prepare(s):
        rows_now = metas[s]
        ids_down = lax.broadcasted_iota(jnp.int32, (slots, tokens), 0).astype(f32)
        ids_down = ids_down + (z * slots).astype(f32)
        table = jnp.zeros((slots, tokens), f32)
        value = jnp.zeros((slots, tokens), f32)
        for k in range(top):
            hit = ids_down == rows_now[k : k + 1]
            table = jnp.where(hit, 1.0, table)
            value = jnp.where(hit, rows_now[top + k : top + k + 1], value)
        tables[s] = table.astype(bf16)
        high = value.astype(bf16)
        weigh[s, :, :tokens] = high
        weigh[s, :, tokens:] = (value - high.astype(f32)).astype(bf16)

    def arrive(code):
        r = code // 2

        def one(i, carry):
            side = i % 2
            k = (code % 2) * (blocks // 2) + i // 2
            s = jnp.where(side == 0, z - r, z + r)
            here = jnp.logical_and(s >= 0, s < layers)
            here = jnp.logical_and(here, jnp.logical_or(r > 0, side == 0))
            far = jnp.logical_and(here, r > 0)
            onward = jnp.logical_and(far, jnp.where(side == 0, z < layers - 1, z > 0))
            s = jnp.clip(s, 0, layers - 1)

            @pl.when(jnp.logical_and(far, k == 0))
            def _():
                meta_copy(z, s).wait_recv()

            @pl.when(jnp.logical_and(here, k == 0))
            def _():
                prepare(s)

            @pl.when(far)
            def _():
                chunk_copy(s, k, 0).wait_recv()

            @pl.when(onward)
            def _():
                chunk_copy(s, k, side).start()

            @pl.when(here)
            def _():
                got = jnp.dot(tables[s], gathered[s, k], preferred_element_type=f32)
                packed[s, k] = got.astype(bf16).reshape(peers, cap, cols)
                for o in far_first:
                    pack_copy(s, k, (me + o) % peers, me).start()
                own_pack(s, k).start()

            return carry

        lax.fori_loop(0, 2 * (blocks // 2), one, 0)

    def mlp(tall, w_gate, w_up):
        gate = jnp.dot(tall, w_gate[...], preferred_element_type=f32)
        up = jnp.dot(tall, w_up[...], preferred_element_type=f32)
        return (gate / (1.0 + jnp.exp(-gate)) * up).astype(bf16)

    def expert(s):
        def taken(k, carry):
            for o in range(1, peers):
                p = (me + o) % peers
                pack_copy(s, k, p, p).wait_recv()
            own_pack(s, k).wait()
            return carry

        lax.fori_loop(0, blocks, taken, 0)
        tall = jnp.concatenate(
            [arrived[s, k].reshape(slots, cols) for k in range(blocks)], axis=1
        )
        hidden = mlp(tall, eg, eu)
        for k in range(blocks):
            got = jnp.dot(hidden, ed[:, k * cols : (k + 1) * cols], preferred_element_type=f32)
            results[s, k] = got.astype(bf16).reshape(peers, cap, cols)
            for o in far_first:
                back_copy(s, k, (me + o) % peers, me).start()
            own_back(s, k).start()

    def combine(s):
        below = jnp.logical_and(s >= z, z > 0)
        above = jnp.logical_and(s <= z, z < layers - 1)

        def one(k, carry):
            for o in range(1, peers):
                p = (me + o) % peers
                back_copy(s, k, p, p).wait_recv()
            own_back(s, k).wait()
            both = lax.dot_general(
                weigh[s], back[s, k].reshape(slots, cols), (((0,), (0,)), ((), ())),
                preferred_element_type=f32,
            )
            got = both[:tokens] + both[tokens:]

            @pl.when(below)
            def _():
                part_copy(s, k, 0).wait_recv()

            @pl.when(above)
            def _():
                part_copy(s, k, 1).wait_recv()

            @pl.when(s == z)
            def _():
                total = acc[k] + got
                total = total + jnp.where(below, landed[0, s, k].astype(f32), 0.0)
                total = total + jnp.where(above, landed[1, s, k].astype(f32), 0.0)
                out_ref[:, pl.ds(pl.multiple_of(k * cols, cols), cols)] = total.astype(bf16)

            @pl.when(s > z)
            def _():
                total = got + jnp.where(below, landed[0, s, k].astype(f32), 0.0)
                part[s, k] = total.astype(bf16)
                part_copy(s, k, 0).start()

            @pl.when(s < z)
            def _():
                total = got + jnp.where(above, landed[1, s, k].astype(f32), 0.0)
                part[s, k] = total.astype(bf16)
                part_copy(s, k, 1).start()

            return carry

        lax.fori_loop(0, blocks, one, 0)

    def shared():
        for load in loads[8:11]:
            load.wait()
        tall = jnp.concatenate([gathered[z, k] for k in range(blocks)], axis=1)
        hidden = mlp(tall, sg, su)
        for k in range(blocks):
            acc[k] = acc[k] + jnp.dot(
                hidden, sd[:, k * cols : (k + 1) * cols], preferred_element_type=f32
            )
        for load in loads[11:]:
            load.wait()

    plans = [steps_of(s, layers) for s in range(layers)]
    count = max(len(plan) for plan in plans)
    kinds, values = [], []
    for t in range(count):
        kind, value = jnp.int32(NOP), jnp.int32(0)
        for s, plan in enumerate(plans):
            if t < len(plan):
                kind = jnp.where(z == s, plan[t][0], kind)
                value = jnp.where(z == s, plan[t][1], value)
        kinds.append(kind)
        values.append(value)

    def step(t, carry):
        kind, value = jnp.int32(NOP), jnp.int32(0)
        for i in range(count):
            kind = jnp.where(t == i, kinds[i], kind)
            value = jnp.where(t == i, values[i], value)
        for number, act in (
            (ARRIVE, arrive), (EXPERT, expert), (COMBINE, combine),
        ):
            @pl.when(kind == number)
            def _():
                act(value)

        @pl.when(kind == SHARED)
        def _():
            shared()

        return carry

    lax.fori_loop(0, count, step, 0)

    def drain(i, carry):
        s = i // blocks
        k = i % blocks

        @pl.when(jnp.logical_and(s <= z, z < layers - 1))
        def _():
            chunk_copy(s, k, 0).wait_send()

        @pl.when(jnp.logical_and(s >= z, z > 0))
        def _():
            chunk_copy(s, k, 1).wait_send()

        for o in range(1, peers):
            p = (me + o) % peers
            pack_copy(s, k, p, me).wait_send()
            back_copy(s, k, p, me).wait_send()

        @pl.when(s != z)
        def _():
            part_copy(s, k, 0).wait_send()

        return carry

    lax.fori_loop(0, layers * blocks, drain, 0)
    for o in range(1, layers):
        meta_copy((z + o) % layers, z).wait_send()
    for o in range(1, cores):
        swap_copy((core + o) % cores, core).wait_send()

    @pl.when(sp < size_sp - 1)
    def _():
        halo_copy().wait_send()


def on_device(
    residual,
    pool_input,
    group_maps,
    pool_scale,
    out_proj,
    norm_gain,
    shared_gate,
    shared_up,
    shared_down,
    expert_gate,
    expert_up,
    expert_down,
    expert_ids,
    route_score,
):
    rows, channels = pool_input.shape
    group_width = group_maps.shape[1]
    tokens, top = expert_ids.shape
    width = residual.shape[1]
    size_sp = lax.axis_size("sp")
    cores = lax.axis_size("tp")
    experts = size_sp * cores
    capacity = 3 * tokens * top // (2 * experts)
    cap = -(-capacity // 8) * 8
    layers = layer_count(size_sp)
    peers = experts // layers
    slots = peers * cap
    hidden_width = shared_gate.shape[1]
    expert_width = expert_gate.shape[2]
    cols = min(width, 512)
    blocks = width // cols
    bf16, f32 = jnp.bfloat16, jnp.float32
    dma = pltpu.SemaphoreType.DMA
    routed = (layers, blocks, peers, cap, cols)
    chunks = (layers, blocks, tokens, cols)
    return pl.pallas_call(
        functools.partial(layer_kernel, layers, peers, cores, cap),
        out_shape=jax.ShapeDtypeStruct((tokens, width), bf16),
        in_specs=[pl.BlockSpec(memory_space=pl.ANY)] * 14,
        out_specs=pl.BlockSpec(memory_space=pltpu.VMEM),
        scratch_shapes=[
            pltpu.VMEM((tokens, width), bf16),
            pltpu.VMEM((rows, channels), bf16),
            pltpu.VMEM((halo_rows, channels), bf16),
            pltpu.VMEM((channels // group_width, group_width, group_width), bf16),
            pltpu.VMEM((1, channels), f32),
            pltpu.VMEM((1, width), f32),
            pltpu.VMEM((tokens, top), jnp.int32),
            pltpu.VMEM((tokens, top), f32),
            pltpu.VMEM((cores, rows // cores, channels), bf16),
            pltpu.VMEM((cores, rows // cores, channels), bf16),
            pltpu.VMEM(out_proj.shape, bf16),
            pltpu.VMEM(chunks, bf16),
            pltpu.VMEM((layers, 2 * top, tokens), f32),
            pltpu.VMEM((layers, slots, tokens), bf16),
            pltpu.VMEM((layers, slots, 2 * tokens), bf16),
            pltpu.VMEM(routed, bf16),
            pltpu.VMEM(routed, bf16),
            pltpu.VMEM(routed, bf16),
            pltpu.VMEM(routed, bf16),
            pltpu.VMEM(chunks, bf16),
            pltpu.VMEM((2,) + chunks, bf16),
            pltpu.VMEM((blocks, tokens, cols), f32),
            pltpu.VMEM((width, hidden_width), bf16),
            pltpu.VMEM((width, hidden_width), bf16),
            pltpu.VMEM((hidden_width, width), bf16),
            pltpu.VMEM((width, expert_width), bf16),
            pltpu.VMEM((width, expert_width), bf16),
            pltpu.VMEM((expert_width, width), bf16),
            dma((14,)),
            dma((2,)),
            dma((cores,)),
            dma((cores,)),
            dma((2, layers, blocks)),
            dma((layers, blocks)),
            dma((layers,)),
            dma((layers,)),
            dma((layers, blocks, peers)),
            dma((layers, blocks, peers)),
            dma((layers, blocks, peers)),
            dma((layers, blocks, peers)),
            dma((layers, blocks)),
            dma((2, layers, blocks)),
        ],
        compiler_params=pltpu.CompilerParams(
            collective_id=0, has_side_effects=True, vmem_limit_bytes=60 * 1024 * 1024
        ),
    )(
        residual,
        pool_input,
        group_maps,
        pool_scale.reshape(1, -1),
        out_proj,
        norm_gain.reshape(1, -1),
        shared_gate,
        shared_up,
        shared_down,
        expert_gate,
        expert_up,
        expert_down,
        expert_ids,
        route_score,
    )


def solution(mesh):
    in_specs = (
        P(("sp", "tp"), None),
        P("sp", "tp"),
        P(),
        P(),
        P(),
        P(),
        P(),
        P(),
        P(),
        P(("sp", "tp"), None, None),
        P(("sp", "tp"), None, None),
        P(("sp", "tp"), None, None),
        P(("sp", "tp"), None),
        P(("sp", "tp"), None),
    )
    out_specs = P(("sp", "tp"), None)
    return jax.shard_map(
        on_device, mesh=mesh, in_specs=in_specs, out_specs=out_specs, check_vma=False
    )
```

time: 130 us -> 105 us (0.81)
  the two profiles are of different devices: /device:TPU:29 before, /device:TPU:0 now
where the time goes in v1:
time: 105 us
  Pallas kernels  100 us (95%)
  local copies, waits for them, and re-layouts  4.7 us (4%)
    pallas_call x1, Pallas kernels, on_device(): pl.pallas_call(functools.partial(layer_kernel, layers, peers, cores, cap)...  100 us
    unnamed x3, local copies, waits for them, and re-layouts  4.7 us

profile of v1, /device:TPU:0, one launch (start us, length us, event | category | flops | bytes accessed | tf_op | source)
XLA Modules:
  0.0 104.7 jit_solution(9767551648358911365)
XLA Ops:
  0.0 1.4 %copy.15.ids_hbm = s32[128,4]{1,0:T(8,128)} copy(s32[128,4]{0,1:T(4,128)} %param.26) | data formatting | bytes 4096 | tf_op args[12]
  1.4 1.4 %copy.16.score_hbm = f32[128,4]{1,0:T(8,128)} copy(f32[128,4]{0,1:T(4,128)} %param.27) | data formatting | bytes 4096 | tf_op args[13]
  2.8 100.0 %shard_map.136 = bf16[128,2048]{1,0:T(8,128)(2,1)} custom-call(bf16[128,2048]{1,0:T(8,128)(2,1)} %residual_hbm.1, bf16[256,512]{1,0:T(8,128)(2,1)} %pool_hbm.1, bf16[8,128,128]{2,1,0:T(8,128)(2,1)} %maps_hbm.1, f32[1,1024]{1,0:T(1,128)} %bitcast.3, bf16[1024,2048]{1,0:T(8,128)(2,1)} %proj_hbm.1, f32[1,2048]{1,0:T(1,128)} %bitcast.2, ...), custom_call_target="tpu_custom_call" | custom-call | tf_op jit(solution)/shard_map/pallas_call | solution.py:588
  102.8 1.9 %copy.18 = bf16[128,2048]{1,0:T(8,128)(2,1)} copy(bf16[128,2048]{1,0:T(8,128)(2,1)} %shard_map.136) | data formatting | bytes 1048576

commit v2 on v1

v2 whole, which is shorter than its diff:
```python
import functools
import math

import jax
import jax.numpy as jnp
from jax import lax
from jax.experimental import pallas as pl
from jax.experimental.pallas import tpu as pltpu
from jax.sharding import PartitionSpec as P

windows = (2, 4, 8, 16)
epsilon = 1e-06
routed_scale = 2.5
halo_rows = 16


def layer_count(size_sp):
    return max(d for d in range(1, math.isqrt(size_sp) + 1) if size_sp % d == 0)


END = " ".join(
    (
        "a00 a01 a02 a03",
        "a10 a11 a12 a13",
        "a20 a21 e1 b10",
        "a22 a23 a30 s",
        "b11 c10 a31 a32",
        "e2 a33 c11 b20",
        "b21 e3 c20 b30",
        "c21 b31 e0 b32",
        "b33 b22 b23 c30",
        "b00 c31 b12 c32",
        "c33 b13 b01 c22",
        "c23 c12 b02 c00",
        "b03 c13 c01 c02",
        "c03",
    )
)
MIDDLE = " ".join(
    (
        "a00 a01 a02 a03",
        "a10 a11 a12 a13",
        "e1 a20 a21 a22",
        "e0 b10 a23 e2",
        "b20 b00 b21 e3",
        "b01 b30 b31 b22",
        "c20 b32 b33 c21",
        "s c10 b02 c30",
        "b11 b03 c31 b23",
        "c00 c32 c01 c33",
        "c11 c02 b12 c22",
        "c03 b13 c23 c12",
        "c13",
    )
)


def steps_of(z, layers, blocks):
    last = layers - 1
    if (layers, blocks) == (4, 4):
        steps = []
        for word in (END if z in (0, last) else MIDDLE).split():
            numbers = [int(digit) for digit in word[1:]]
            if word[0] in "ebc" and 2 * z > last:
                numbers[0] = last - numbers[0]
            steps.append((word[0], *numbers))
        return steps
    at = lambda r: sorted({s for s in (z - r, z + r) if 0 <= s < layers})
    reach = max(z, last - z)
    span = range(blocks)
    steps = [("a", 0, k) for k in span] + [("s",)]
    for r in range(1, reach + 2):
        if r <= reach:
            steps += [("a", r, k) for k in span]
        for s in at(r - 1):
            steps += [("e", s)] + [("b", s, k) for k in span]
    for r in range(reach, -1, -1):
        steps += [("c", s, k) for s in at(r) for k in span]
    return steps


def code_of(step, layers, blocks):
    area = layers * blocks
    base = {"a": 0, "b": area, "c": 2 * area, "e": 3 * area, "s": 3 * area + layers}[step[0]]
    if len(step) == 3:
        return base + step[1] * blocks + step[2]
    return base + sum(step[1:])


def layer_kernel(
    layers,
    peers,
    cores,
    cap,
    residual_hbm,
    pool_hbm,
    maps_hbm,
    scale_hbm,
    proj_hbm,
    gain_hbm,
    sg_hbm,
    su_hbm,
    sd_hbm,
    eg_hbm,
    eu_hbm,
    ed_hbm,
    ids_hbm,
    score_hbm,
    out_hbm,
    residual,
    pool,
    halo,
    head,
    maps,
    scale,
    gain,
    ids,
    score,
    mixed,
    swapped,
    proj,
    gathered,
    metas,
    tables,
    weigh,
    packed,
    arrived,
    results,
    back,
    part,
    landed,
    acc,
    final,
    sg,
    su,
    sd,
    eg,
    eu,
    ed,
    w_sem,
    o_sem,
    h_send,
    h_recv,
    x_send,
    x_recv,
    z_send,
    z_recv,
    m_send,
    m_recv,
    a_send,
    a_recv,
    b_send,
    b_recv,
    c_send,
    c_recv,
):
    per_layer = peers // cores
    sp = lax.axis_index("sp")
    size_sp = layers * per_layer
    core = lax.axis_index("tp")
    z = sp // per_layer
    q = sp % per_layer
    me = q * cores + core
    blocks, tokens, cols = acc.shape
    width = blocks * cols
    slots = peers * cap
    top = ids.shape[0]
    rows, channels = pool.shape
    group_width = maps.shape[1]
    groups_here = channels // group_width
    area = layers * blocks
    f32, bf16 = jnp.float32, jnp.bfloat16

    def in_column(s):
        return (s * per_layer + q, core)

    def in_layer(p):
        return (z * per_layer + p // cores, p % cores)

    def remote(src, dst, send, recv, to):
        return pltpu.make_async_remote_copy(
            src_ref=src,
            dst_ref=dst,
            send_sem=send,
            recv_sem=recv,
            device_id=to,
            device_id_type=pl.DeviceIdType.MESH,
        )

    def tell(to):
        pl.semaphore_signal(
            pltpu.get_barrier_semaphore(), inc=1, device_id=to,
            device_id_type=pl.DeviceIdType.MESH,
        )

    pairs = (
        (pool_hbm, pool),
        (ids_hbm, ids),
        (score_hbm, score),
        (maps_hbm, maps),
        (scale_hbm, scale),
        (proj_hbm, proj),
        (residual_hbm, residual),
        (gain_hbm, gain),
        (sg_hbm, sg),
        (su_hbm, su),
        (sd_hbm, sd),
        (eg_hbm.at[0], eg),
        (eu_hbm.at[0], eu),
        (ed_hbm.at[0], ed),
    )
    loads = [pltpu.make_async_copy(a, b, w_sem.at[i]) for i, (a, b) in enumerate(pairs)]
    for load in loads[:5]:
        load.start()
    for o in range(1, layers):
        tell(in_column((z + o) % layers))
    for o in range(1, peers):
        tell(in_layer((me + o) % peers))

    takes_halo = jnp.logical_and(sp > 0, core == 0)
    gives_halo = sp < size_sp - 1

    @pl.when(takes_halo)
    def _():
        for c in range(cores):
            tell((sp - 1, c))

    for load in loads[5:8]:
        load.start()

    loads[1].wait()
    loads[2].wait()
    experts = layers * peers
    ids_now = ids[...]
    score_now = score[...]
    expert_at = lax.broadcasted_iota(jnp.int32, (experts, tokens), 0)
    named = [(ids_now[k : k + 1] == expert_at).astype(f32) for k in range(top)]
    named_any = functools.reduce(jnp.add, named).astype(bf16)
    earlier = (
        lax.broadcasted_iota(jnp.int32, (tokens, tokens), 0)
        < lax.broadcasted_iota(jnp.int32, (tokens, tokens), 1)
    ).astype(bf16)
    rank = jnp.dot(named_any, earlier, preferred_element_type=f32)
    shares = score_now / jnp.sum(score_now, axis=0, keepdims=True) * routed_scale
    slot = [
        ids_now[k : k + 1].astype(f32) * cap + jnp.sum(rank * named[k], axis=0, keepdims=True)
        for k in range(top)
    ]
    metas[z] = jnp.concatenate(slot + [shares], axis=0)

    half = rows // cores

    def mix(before, own, start, c):
        place = start + lax.broadcasted_iota(jnp.int32, (own.shape[0], group_width), 0)
        out = []
        for g in range(groups_here):
            lanes = slice(g * group_width, (g + 1) * group_width)
            here = own[:, lanes]
            total = jnp.concatenate([before[:, lanes], here], axis=0)
            span = 1
            while span < windows[g % 4]:
                total = total + pltpu.roll(total, span, 0)
                span = span * 2
            divisor = jnp.minimum(place + 1, span).astype(f32)
            contrast = (total[halo_rows:] / divisor - here).astype(bf16)
            group = c * groups_here + g
            mapped = jnp.dot(contrast, maps[group], preferred_element_type=f32)
            out.append((mapped * scale[group]).astype(bf16))
        return jnp.concatenate(out, axis=1)

    for i in (0, 3, 4):
        loads[i].wait()
    for c in range(cores):
        start = c * half
        before = pool[max(start - halo_rows, 0) : max(start, halo_rows)].astype(f32)
        if c == 0:
            before = jnp.zeros_like(before)
        mixed[c] = mix(before, pool[start : start + half].astype(f32), sp * rows + start, core)

    pl.semaphore_wait(
        pltpu.get_barrier_semaphore(),
        layers - 1 + peers - 1 + jnp.where(gives_halo, 1, 0),
    )

    def halo_copy(source):
        return remote(
            pool.at[pl.ds(rows - halo_rows, halo_rows)], halo.at[source], h_send.at[0],
            h_recv.at[0, source], (jnp.minimum(sp + 1, size_sp - 1), 0),
        )

    def head_copy(source):
        return remote(
            pool.at[pl.ds(0, halo_rows)], head.at[source], h_send.at[1],
            h_recv.at[1, source], (sp, 0),
        )

    def swap_copy(p, source):
        return remote(
            mixed.at[p], swapped.at[source], x_send.at[p], x_recv.at[source], (sp, p)
        )

    @pl.when(gives_halo)
    def _():
        halo_copy(core).start()

    for o in range(1, cores):
        swap_copy((core + o) % cores, core).start()

    gives_head = jnp.logical_and(sp > 0, core > 0)

    @pl.when(gives_head)
    def _():
        head_copy(core).start()

    def meta_copy(target, source):
        return remote(
            metas.at[source], metas.at[source], m_send.at[target], m_recv.at[source],
            in_column(target),
        )

    for o in range(1, layers):
        meta_copy((z + o) % layers, z).start()
    for load in loads[8:11]:
        load.start()

    def neighbour(side):
        return in_column(jnp.clip(jnp.where(side == 0, z + 1, z - 1), 0, layers - 1))

    def chunk_copy(s, k, side):
        return remote(
            gathered.at[s, k], gathered.at[s, k], z_send.at[side, s], z_recv.at[s, k],
            neighbour(side),
        )

    def pack_copy(s, k, p, source):
        return remote(
            packed.at[s, k, p], arrived.at[s, k, source], a_send.at[s],
            a_recv.at[s], in_layer(p),
        )

    def back_copy(s, k, p, source):
        return remote(
            results.at[s, k, p], back.at[s, k, source], b_send.at[s],
            b_recv.at[s, k], in_layer(p),
        )

    def own_pack(s, k):
        return pltpu.make_async_copy(
            packed.at[s, k, me], arrived.at[s, k, me], a_recv.at[s]
        )

    def own_back(s, k):
        return pltpu.make_async_copy(
            results.at[s, k, me], back.at[s, k, me], b_recv.at[s, k]
        )

    def part_copy(s, k, side):
        slot = jnp.where(jnp.logical_and(side == 1, s == z - 1), layers, s)
        return remote(
            part.at[s, k], landed.at[slot, k], c_send.at[s], c_recv.at[slot, k],
            neighbour(side),
        )

    def wait_bytes(ref, sem):
        pltpu.make_async_copy(ref, ref, sem).wait()

    far_first = sorted(range(1, peers), key=lambda o: (o % cores, -o % 3, o))

    for load in loads[11:]:
        load.start()
    for o in range(1, cores):
        p = (core + o) % cores
        swap_copy(p, p).wait_recv()

    @pl.when(takes_halo)
    def _():
        for c in range(cores):
            halo_copy(c).wait_recv()
            own = pool[:halo_rows]
            if c > 0:
                head_copy(c).wait_recv()
                own = head[c]
            fixed = mix(halo[c].astype(f32), own.astype(f32), sp * rows, c)
            if c == 0:
                mixed[0, :halo_rows] = fixed
            else:
                swapped[c, :halo_rows] = fixed

    for load in loads[5:8]:
        load.wait()

    def channels_of(c):
        return pl.ds(pl.multiple_of(c * channels, channels), channels)

    for k in range(blocks):
        lanes = slice(k * cols, (k + 1) * cols)
        total = residual[:, lanes].astype(f32) + jnp.dot(
            mixed[core], proj[channels_of(core), lanes], preferred_element_type=f32
        )
        for o in range(1, cores):
            p = (core + o) % cores
            total = total + jnp.dot(
                swapped[p], proj[channels_of(p), lanes], preferred_element_type=f32
            )
        acc[k] = total
    squares = jnp.zeros((tokens, 1), f32)
    for k in range(blocks):
        settled = acc[k].astype(bf16).astype(f32)
        acc[k] = settled
        squares = squares + jnp.sum(settled * settled, axis=1, keepdims=True)
    inverse = lax.rsqrt(squares / width + epsilon)
    for k in range(blocks):
        gathered[z, k] = (acc[k] * inverse * gain[:, k * cols : (k + 1) * cols]).astype(bf16)

        @pl.when(z < layers - 1)
        def _():
            chunk_copy(z, k, 0).start()

        @pl.when(z > 0)
        def _():
            chunk_copy(z, k, 1).start()

    def prepare(s):
        rows_now = metas[s]
        ids_down = lax.broadcasted_iota(jnp.int32, (slots, tokens), 0).astype(f32)
        ids_down = ids_down + (z * slots).astype(f32)
        table = jnp.zeros((slots, tokens), f32)
        value = jnp.zeros((slots, tokens), f32)
        for k in range(top):
            hit = ids_down == rows_now[k : k + 1]
            table = jnp.where(hit, 1.0, table)
            value = jnp.where(hit, rows_now[top + k : top + k + 1], value)
        tables[s] = table.astype(bf16)
        high = value.astype(bf16)
        weigh[s, :, :tokens] = high
        weigh[s, :, tokens:] = (value - high.astype(f32)).astype(bf16)

    def arrive(r, k):
        def one(side, carry):
            s = jnp.where(side == 0, z - r, z + r)
            here = jnp.logical_and(s >= 0, s < layers)
            here = jnp.logical_and(here, jnp.logical_or(r > 0, side == 0))
            far = jnp.logical_and(here, r > 0)
            onward = jnp.logical_and(far, jnp.where(side == 0, z < layers - 1, z > 0))
            s = jnp.clip(s, 0, layers - 1)

            @pl.when(far)
            def _():
                chunk_copy(s, k, 0).wait_recv()

            @pl.when(onward)
            def _():
                chunk_copy(s, k, side).start()

            @pl.when(jnp.logical_and(far, k == 0))
            def _():
                meta_copy(z, s).wait_recv()

            @pl.when(jnp.logical_and(here, k == 0))
            def _():
                prepare(s)

            @pl.when(here)
            def _():
                got = jnp.dot(tables[s], gathered[s, k], preferred_element_type=f32)
                packed[s, k] = got.astype(bf16).reshape(peers, cap, cols)
                for o in far_first:
                    pack_copy(s, k, (me + o) % peers, me).start()
                own_pack(s, k).start()

            return carry

        lax.fori_loop(0, 2, one, 0)

    def mlp(tall, w_gate, w_up):
        gate = jnp.dot(tall, w_gate[...], preferred_element_type=f32)
        up = jnp.dot(tall, w_up[...], preferred_element_type=f32)
        return (gate / (1.0 + jnp.exp(-gate)) * up).astype(bf16)

    def expert(s):
        wait_bytes(arrived.at[s], a_recv.at[s])
        tall = jnp.concatenate(
            [arrived[s, k].reshape(slots, cols) for k in range(blocks)], axis=1
        )
        hidden = mlp(tall, eg, eu)
        for k in range(blocks):
            got = jnp.dot(hidden, ed[:, k * cols : (k + 1) * cols], preferred_element_type=f32)
            results[s, k] = got.astype(bf16).reshape(peers, cap, cols)

    def give_back(s, k):
        for o in far_first:
            back_copy(s, k, (me + o) % peers, me).start()
        own_back(s, k).start()

    def out_copy(k):
        lanes = pl.ds(pl.multiple_of(k * cols, cols), cols)
        return pltpu.make_async_copy(final.at[k], out_hbm.at[:, lanes], o_sem.at[k])

    def combine(s, k):
        below = jnp.logical_and(s >= z, z > 0)
        above = jnp.logical_and(s <= z, z < layers - 1)
        over = jnp.where(s == z, layers, s)
        wait_bytes(back.at[s, k], b_recv.at[s, k])
        both = lax.dot_general(
            weigh[s], back[s, k].reshape(slots, cols), (((0,), (0,)), ((), ())),
            preferred_element_type=f32,
        )
        got = both[:tokens] + both[tokens:]

        @pl.when(below)
        def _():
            wait_bytes(landed.at[s, k], c_recv.at[s, k])

        @pl.when(above)
        def _():
            wait_bytes(landed.at[over, k], c_recv.at[over, k])

        got = got + jnp.where(below, landed[s, k].astype(f32), 0.0)
        got = got + jnp.where(above, landed[over, k].astype(f32), 0.0)

        @pl.when(s == z)
        def _():
            final[k] = (acc[k] + got).astype(bf16)
            out_copy(k).start()

        @pl.when(s != z)
        def _():
            part[s, k] = got.astype(bf16)
            part_copy(s, k, jnp.where(s > z, 0, 1)).start()

    def shared():
        for load in loads[8:11]:
            load.wait()
        tall = jnp.concatenate([gathered[z, k] for k in range(blocks)], axis=1)
        hidden = mlp(tall, sg, su)
        for k in range(blocks):
            acc[k] = acc[k] + jnp.dot(
                hidden, sd[:, k * cols : (k + 1) * cols], preferred_element_type=f32
            )

    plans = [
        [code_of(step, layers, blocks) for step in steps_of(s, layers, blocks)]
        for s in range(layers)
    ]
    nothing = 3 * area + layers + 1
    base = 1 << nothing.bit_length()
    per_word = 30 // nothing.bit_length()
    count = -(-max(len(plan) for plan in plans) // per_word)
    words = []
    for i in range(count):
        word = jnp.int32(0)
        for s, plan in enumerate(plans):
            codes = plan[i * per_word : (i + 1) * per_word]
            codes = codes + [nothing] * (per_word - len(codes))
            packed_codes = sum(code * base**j for j, code in enumerate(codes))
            word = jnp.where(z == s, packed_codes, word)
        words.append(word)

    def act(code):
        number = code % area
        s = number // blocks
        k = number % blocks

        @pl.when(code < area)
        def _():
            arrive(s, k)

        @pl.when(code == 2 * blocks - 1)
        def _():
            for load in loads[11:]:
                load.wait()

        @pl.when(jnp.logical_and(code >= area, code < 2 * area))
        def _():
            give_back(s, k)

        @pl.when(jnp.logical_and(code >= 2 * area, code < 3 * area))
        def _():
            combine(s, k)

        @pl.when(jnp.logical_and(code >= 3 * area, code < 3 * area + layers))
        def _():
            expert(code - 3 * area)

        @pl.when(code == 3 * area + layers)
        def _():
            shared()

    def several(i, carry):
        word = words[0]
        for j in range(1, count):
            word = jnp.where(i == j, words[j], word)

        def single(j, word):
            act(word % base)
            return word // base

        lax.fori_loop(0, per_word, single, word)
        return carry

    lax.fori_loop(0, count, several, 0)

    def drain(s, carry):
        @pl.when(jnp.logical_and(s <= z, z < layers - 1))
        def _():
            wait_bytes(gathered.at[s], z_send.at[0, s])

        @pl.when(jnp.logical_and(s >= z, z > 0))
        def _():
            wait_bytes(gathered.at[s], z_send.at[1, s])

        wait_bytes(packed.at[s, :, pl.ds(1, peers - 1)], a_send.at[s])
        wait_bytes(results.at[s, :, pl.ds(1, peers - 1)], b_send.at[s])

        @pl.when(s != z)
        def _():
            wait_bytes(part.at[s], c_send.at[s])

        return carry

    lax.fori_loop(0, layers, drain, 0)
    for o in range(1, layers):
        meta_copy((z + o) % layers, z).wait_send()
    for o in range(1, cores):
        swap_copy((core + o) % cores, core).wait_send()

    @pl.when(gives_halo)
    def _():
        halo_copy(core).wait_send()

    @pl.when(gives_head)
    def _():
        head_copy(core).wait_send()

    for k in range(blocks):
        out_copy(k).wait()


def on_device(
    residual,
    pool_input,
    group_maps,
    pool_scale,
    out_proj,
    norm_gain,
    shared_gate,
    shared_up,
    shared_down,
    expert_gate,
    expert_up,
    expert_down,
    expert_ids,
    route_score,
):
    rows, channels = pool_input.shape
    group_width = group_maps.shape[1]
    tokens, top = expert_ids.shape
    width = residual.shape[1]
    size_sp = lax.axis_size("sp")
    cores = lax.axis_size("tp")
    experts = size_sp * cores
    capacity = 3 * tokens * top // (2 * experts)
    cap = -(-capacity // 8) * 8
    layers = layer_count(size_sp)
    peers = experts // layers
    slots = peers * cap
    hidden_width = shared_gate.shape[1]
    expert_width = expert_gate.shape[2]
    cols = min(width, 512)
    blocks = width // cols
    bf16, f32 = jnp.bfloat16, jnp.float32
    dma = pltpu.SemaphoreType.DMA
    routed = (layers, blocks, peers, cap, cols)
    chunks = (layers, blocks, tokens, cols)
    return pl.pallas_call(
        functools.partial(layer_kernel, layers, peers, cores, cap),
        out_shape=jax.ShapeDtypeStruct((tokens, width), bf16),
        in_specs=[pl.BlockSpec(memory_space=pltpu.HBM)] * 14,
        out_specs=pl.BlockSpec(memory_space=pltpu.HBM),
        scratch_shapes=[
            pltpu.VMEM((tokens, width), bf16),
            pltpu.VMEM((rows, channels), bf16),
            pltpu.VMEM((cores, halo_rows, channels), bf16),
            pltpu.VMEM((cores, halo_rows, channels), bf16),
            pltpu.VMEM(group_maps.shape, bf16),
            pltpu.VMEM((group_maps.shape[0], 1, group_width), f32),
            pltpu.VMEM((1, width), f32),
            pltpu.VMEM((top, tokens), jnp.int32),
            pltpu.VMEM((top, tokens), f32),
            pltpu.VMEM((cores, rows // cores, channels), bf16),
            pltpu.VMEM((cores, rows // cores, channels), bf16),
            pltpu.VMEM(out_proj.shape, bf16),
            pltpu.VMEM(chunks, bf16),
            pltpu.VMEM((layers, 2 * top, tokens), f32),
            pltpu.VMEM((layers, slots, tokens), bf16),
            pltpu.VMEM((layers, slots, 2 * tokens), bf16),
            pltpu.VMEM(routed, bf16),
            pltpu.VMEM(routed, bf16),
            pltpu.VMEM(routed, bf16),
            pltpu.VMEM(routed, bf16),
            pltpu.VMEM(chunks, bf16),
            pltpu.VMEM((layers + 1, blocks, tokens, cols), bf16),
            pltpu.VMEM((blocks, tokens, cols), f32),
            pltpu.VMEM((blocks, tokens, cols), bf16),
            pltpu.VMEM((width, hidden_width), bf16),
            pltpu.VMEM((width, hidden_width), bf16),
            pltpu.VMEM((hidden_width, width), bf16),
            pltpu.VMEM((width, expert_width), bf16),
            pltpu.VMEM((width, expert_width), bf16),
            pltpu.VMEM((expert_width, width), bf16),
            dma((14,)),
            dma((blocks,)),
            dma((2,)),
            dma((2, cores)),
            dma((cores,)),
            dma((cores,)),
            dma((2, layers)),
            dma((layers, blocks)),
            dma((layers,)),
            dma((layers,)),
            dma((layers,)),
            dma((layers,)),
            dma((layers,)),
            dma((layers, blocks)),
            dma((layers,)),
            dma((layers + 1, blocks)),
        ],
        compiler_params=pltpu.CompilerParams(
            collective_id=0, has_side_effects=True, vmem_limit_bytes=56 * 1024 * 1024
        ),
    )(
        residual,
        pool_input,
        group_maps,
        pool_scale.reshape(-1, 1, group_width),
        out_proj,
        norm_gain.reshape(1, -1),
        shared_gate,
        shared_up,
        shared_down,
        expert_gate,
        expert_up,
        expert_down,
        expert_ids.T,
        route_score.T,
    )


def solution(mesh):
    in_specs = (
        P(("sp", "tp"), None),
        P("sp", "tp"),
        P(),
        P(),
        P(),
        P(),
        P(),
        P(),
        P(),
        P(("sp", "tp"), None, None),
        P(("sp", "tp"), None, None),
        P(("sp", "tp"), None, None),
        P(("sp", "tp"), None),
        P(("sp", "tp"), None),
    )
    out_specs = P(("sp", "tp"), None)
    return jax.shard_map(
        on_device, mesh=mesh, in_specs=in_specs, out_specs=out_specs, check_vma=False
    )
```

time: 105 us -> 85.8 us (0.82)
  Pallas kernels: 100 us -> 83.7 us
  local copies, waits for them, and re-layouts: 4.7 us -> 1.88 us
    pallas_call x1, Pallas kernels: 100 us -> 83.7 us  [on_device(): pl.pallas_call(functools.partial(layer_kernel, layers, peers, cores, cap)...]
    unnamed x3 -> x1, local copies, waits for them, and re-layouts: 4.7 us -> 1.88 us
where the time goes in v2:
time: 85.8 us; the launch traced here: 85.6 us
  Pallas kernels  83.7 us (98%)
  local copies, waits for them, and re-layouts  1.88 us (2%)
    pallas_call x1, Pallas kernels, on_device(): pl.pallas_call(functools.partial(layer_kernel, layers, peers, cores, cap)...  83.7 us
    unnamed x1, local copies, waits for them, and re-layouts  1.88 us

profile of v2, /device:TPU:0, one launch (start us, length us, event | category | flops | bytes accessed | tf_op | source)
XLA Modules:
  0.0 85.6 jit_solution(12216565698521472776)
XLA Ops:
  0.0 83.7 %shard_map.136 = bf16[128,2048]{1,0:T(8,128)(2,1)} custom-call(bf16[128,2048]{1,0:T(8,128)(2,1)} %residual_hbm.1, bf16[256,512]{1,0:T(8,128)(2,1)} %pool_hbm.1, bf16[8,128,128]{2,1,0:T(8,128)(2,1)} %maps_hbm.1, f32[8,1,128]{2,1,0:T(1,128)} %bitcast.5, bf16[1024,2048]{1,0:T(8,128)(2,1)} %proj_hbm.1, f32[1,2048]{1,0:T(1,128)} %bitcast.4, ...), custom_call_target="tpu_custom_call" | custom-call | tf_op jit(solution)/shard_map/pallas_call | solution.py:675
  83.8 1.9 %copy.16 = bf16[128,2048]{1,0:T(8,128)(2,1)} copy(bf16[128,2048]{1,0:T(8,128)(2,1)} %shard_map.136) | data formatting | bytes 1048576

commit v3 on v2

--- a/solution.py
+++ b/solution.py
@@ -106,7 +106,7 @@
     ed_hbm,
     ids_hbm,
     score_hbm,
-    out_hbm,
+    out_ref,
     residual,
     pool,
     halo,
@@ -130,7 +130,6 @@
     part,
     landed,
     acc,
-    final,
     sg,
     su,
     sd,
@@ -138,7 +137,6 @@
     eu,
     ed,
     w_sem,
-    o_sem,
     h_send,
     h_recv,
     x_send,
@@ -492,10 +490,6 @@
             back_copy(s, k, (me + o) % peers, me).start()
         own_back(s, k).start()
 
-    def out_copy(k):
-        lanes = pl.ds(pl.multiple_of(k * cols, cols), cols)
-        return pltpu.make_async_copy(final.at[k], out_hbm.at[:, lanes], o_sem.at[k])
-
     def combine(s, k):
         below = jnp.logical_and(s >= z, z > 0)
         above = jnp.logical_and(s <= z, z < layers - 1)
@@ -520,8 +514,8 @@
 
         @pl.when(s == z)
         def _():
-            final[k] = (acc[k] + got).astype(bf16)
-            out_copy(k).start()
+            lanes = pl.ds(pl.multiple_of(k * cols, cols), cols)
+            out_ref[:, lanes] = (acc[k] + got).astype(bf16)
 
         @pl.when(s != z)
         def _():
@@ -631,9 +625,6 @@
     @pl.when(gives_head)
     def _():
         head_copy(core).wait_send()
-
-    for k in range(blocks):
-        out_copy(k).wait()
 
 
 def on_device(
@@ -674,9 +665,9 @@
     chunks = (layers, blocks, tokens, cols)
     return pl.pallas_call(
         functools.partial(layer_kernel, layers, peers, cores, cap),
-        out_shape=jax.ShapeDtypeStruct((tokens, width), bf16),
+        out_shape=pltpu.VMEM((tokens, width), bf16),
         in_specs=[pl.BlockSpec(memory_space=pltpu.HBM)] * 14,
-        out_specs=pl.BlockSpec(memory_space=pltpu.HBM),
+        out_specs=pl.BlockSpec(memory_space=pltpu.VMEM),
         scratch_shapes=[
             pltpu.VMEM((tokens, width), bf16),
             pltpu.VMEM((rows, channels), bf16),
@@ -701,7 +692,6 @@
             pltpu.VMEM(chunks, bf16),
             pltpu.VMEM((layers + 1, blocks, tokens, cols), bf16),
             pltpu.VMEM((blocks, tokens, cols), f32),
-            pltpu.VMEM((blocks, tokens, cols), bf16),
             pltpu.VMEM((width, hidden_width), bf16),
             pltpu.VMEM((width, hidden_width), bf16),
             pltpu.VMEM((hidden_width, width), bf16),
@@ -709,7 +699,6 @@
             pltpu.VMEM((width, expert_width), bf16),
             pltpu.VMEM((expert_width, width), bf16),
             dma((14,)),
-            dma((blocks,)),
             dma((2,)),
             dma((2, cores)),
             dma((cores,)),

time: 85.8 us -> 84.2 us (0.981)
  local copies, waits for them, and re-layouts: 1.88 us -> 0.8 us
    unnamed x1, local copies, waits for them, and re-layouts: 1.88 us -> 0.8 us
where the time goes in v3:
time: 84.2 us; the launch traced here: 84.1 us
  Pallas kernels  83.3 us (99%)
    pallas_call x1, Pallas kernels, on_device(): pl.pallas_call(functools.partial(layer_kernel, layers, peers, cores, cap)...  83.3 us

profile of v3, /device:TPU:0, one launch (start us, length us, event | category | flops | bytes accessed | tf_op | source)
XLA Modules:
  0.0 84.1 jit_solution(16909747554427196115)
XLA Ops:
  0.0 83.3 %shard_map.136 = bf16[128,2048]{1,0:T(8,128)(2,1)S(1)} custom-call(bf16[128,2048]{1,0:T(8,128)(2,1)} %residual_hbm.1, bf16[256,512]{1,0:T(8,128)(2,1)} %pool_hbm.1, bf16[8,128,128]{2,1,0:T(8,128)(2,1)} %maps_hbm.1, f32[8,1,128]{2,1,0:T(1,128)} %bitcast.5, bf16[1024,2048]{1,0:T(8,128)(2,1)} %proj_hbm.1, f32[1,2048]{1,0:T(1,128)} %bitcast.4, ...), custom_call_target="tpu_custom_call" | custom-call | tf_op jit(solution)/shard_map/pallas_call | solution.py:666
  83.3 0.8 copy.16

commit v4 on v3

--- a/solution.py
+++ b/solution.py
@@ -22,17 +22,17 @@
     (
         "a00 a01 a02 a03",
         "a10 a11 a12 a13",
-        "a20 a21 e1 b10",
-        "a22 a23 a30 s",
-        "b11 c10 a31 a32",
-        "e2 a33 c11 b20",
-        "b21 e3 c20 b30",
-        "c21 b31 e0 b32",
-        "b33 b22 b23 c30",
-        "b00 c31 b12 c32",
-        "c33 b13 b01 c22",
-        "c23 c12 b02 c00",
-        "b03 c13 c01 c02",
+        "a20 a21 a22 a23",
+        "e1 b10 a30 a31",
+        "b11 e2 c10 b20",
+        "a32 e0 a33 c11",
+        "c20 b21 b22 e3",
+        "b30 b31 b32 b33",
+        "c21 b23 b00 c30",
+        "b01 c31 s c32",
+        "c33 c22 b02 c23",
+        "b12 b13 b03 c00",
+        "c12 c01 c13 c02",
         "c03",
     )
 )
@@ -40,16 +40,16 @@
     (
         "a00 a01 a02 a03",
         "a10 a11 a12 a13",
-        "e1 a20 a21 a22",
-        "e0 b10 a23 e2",
-        "b20 b00 b21 e3",
-        "b01 b30 b31 b22",
-        "c20 b32 b33 c21",
-        "s c10 b02 c30",
-        "b11 b03 c31 b23",
-        "c00 c32 c01 c33",
-        "c11 c02 b12 c22",
-        "c03 b13 c23 c12",
+        "a20 e1 a21 s",
+        "e2 b20 a22 b10",
+        "e0 a23 b00 e3",
+        "b21 b30 b31 b01",
+        "c20 c21 b32 b02",
+        "b11 c30 b33 c31",
+        "c00 b22 c32 b03",
+        "b23 c10 c01 c33",
+        "b12 c02 c22 b13",
+        "c03 c11 c23 c12",
         "c13",
     )
 )

time: 84.2 us -> 83 us (0.986)
  Pallas kernels: 83.3 us -> 82 us
    pallas_call x1, Pallas kernels: 83.3 us -> 82 us  [on_device(): pl.pallas_call(functools.partial(layer_kernel, layers, peers, cores, cap)...]
where the time goes in v4:
time: 83 us; the launch traced here: 82.8 us
  Pallas kernels  82 us (99%)
    pallas_call x1, Pallas kernels, on_device(): pl.pallas_call(functools.partial(layer_kernel, layers, peers, cores, cap)...  82 us

profile of v4, /device:TPU:0, one launch (start us, length us, event | category | flops | bytes accessed | tf_op | source)
XLA Modules:
  0.0 82.8 jit_solution(85770804514240609)
XLA Ops:
  0.0 82.0 %shard_map.136 = bf16[128,2048]{1,0:T(8,128)(2,1)S(1)} custom-call(bf16[128,2048]{1,0:T(8,128)(2,1)} %residual_hbm.1, bf16[256,512]{1,0:T(8,128)(2,1)} %pool_hbm.1, bf16[8,128,128]{2,1,0:T(8,128)(2,1)} %maps_hbm.1, f32[8,1,128]{2,1,0:T(1,128)} %bitcast.5, bf16[1024,2048]{1,0:T(8,128)(2,1)} %proj_hbm.1, f32[1,2048]{1,0:T(1,128)} %bitcast.4, ...), custom_call_target="tpu_custom_call" | custom-call | tf_op jit(solution)/shard_map/pallas_call | solution.py:666
  82.0 0.8 copy.16

commit v5 on v4

--- a/solution.py
+++ b/solution.py
@@ -18,48 +18,87 @@
     return max(d for d in range(1, math.isqrt(size_sp) + 1) if size_sp % d == 0)
 
 
-END = " ".join(
-    (
-        "a00 a01 a02 a03",
-        "a10 a11 a12 a13",
-        "a20 a21 a22 a23",
-        "e1 b10 a30 a31",
-        "b11 e2 c10 b20",
-        "a32 e0 a33 c11",
-        "c20 b21 b22 e3",
-        "b30 b31 b32 b33",
-        "c21 b23 b00 c30",
-        "b01 c31 s c32",
-        "c33 c22 b02 c23",
-        "b12 b13 b03 c00",
-        "c12 c01 c13 c02",
-        "c03",
-    )
+END = (
+    " ".join(
+        (
+            "a00 a01 a02 a03",
+            "s a10 a11 a12",
+            "a13 a20 a21 a22",
+            "a23 e1 b10 a30",
+            "a31 a32 e2 b20",
+            "a33 c20 c10 b21",
+            "e3 b30 b31 b22",
+            "b32 c21 b33 b11",
+            "c30 b12 e0 c31",
+            "c32 b23 c33 b00",
+            "c22 b13 c00 b01",
+            "b02 b03 c23 c11",
+            "c12 c01 c13 c02",
+            "c03",
+        )
+    ),
+    " ".join(
+        (
+            "a00 a01 a02 a03",
+            "a10 a11 a12 a13",
+            "a20 a21 a22 a23",
+            "e0 e1 b10 e2",
+            "a30 b20 a31 a32",
+            "c10 a33 b21 c20",
+            "b00 e3 b30 c21",
+            "b31 c30 b32 c31",
+            "b33 b11 c32 b22",
+            "b23 b12 c11 c33",
+            "b01 b13 b02 c22",
+            "c23 s c00 c12",
+            "b03 c13 c01 c02",
+            "c03",
+        )
+    ),
 )
-MIDDLE = " ".join(
-    (
-        "a00 a01 a02 a03",
-        "a10 a11 a12 a13",
-        "a20 e1 a21 s",
-        "e2 b20 a22 b10",
-        "e0 a23 b00 e3",
-        "b21 b30 b31 b01",
-        "c20 c21 b32 b02",
-        "b11 c30 b33 c31",
-        "c00 b22 c32 b03",
-        "b23 c10 c01 c33",
-        "b12 c02 c22 b13",
-        "c03 c11 c23 c12",
-        "c13",
-    )
+MIDDLE = (
+    " ".join(
+        (
+            "a00 a01 a02 a03",
+            "a10 a11 a12 a13",
+            "a20 e1 b10 a21",
+            "a22 a23 e2 e0",
+            "b20 b21 e3 b00",
+            "b30 c20 b31 b01",
+            "b02 c21 b32 b11",
+            "b33 c30 c31 c00",
+            "b03 s c32 b22",
+            "c01 b23 c10 b12",
+            "c33 c02 c03 b13",
+            "c22 c23 c11 c12",
+            "c13",
+        )
+    ),
+    " ".join(
+        (
+            "a00 a01 a02 a03",
+            "a10 a11 a12 s",
+            "a13 e1 e2 b20",
+            "a20 a21 a22 a23",
+            "b10 e0 b00 b21",
+            "e3 b30 c20 b31",
+            "b22 b01 b02 c21",
+            "b32 b33 c30 b03",
+            "c31 c32 c00 c01",
+            "c02 b23 c33 b11",
+            "b12 c22 c10 c23",
+            "c03 b13 c11 c12",
+            "c13",
+        )
+    ),
 )
 
 
-def steps_of(z, layers, blocks):
+def steps_of(z, core, layers, blocks):
     last = layers - 1
-    if (layers, blocks) == (4, 4):
+    if (layers, blocks) == (4, 4) and core < len(END):
         steps = []
-        for word in (END if z in (0, last) else MIDDLE).split():
+        for word in (END if z in (0, last) else MIDDLE)[core].split():
             numbers = [int(digit) for digit in word[1:]]
             if word[0] in "ebc" and 2 * z > last:
                 numbers[0] = last - numbers[0]
@@ -130,6 +169,7 @@
     part,
     landed,
     acc,
+    hidden,
     sg,
     su,
     sd,
@@ -226,6 +266,124 @@
     for load in loads[5:8]:
         load.start()
 
+    half = rows // cores
+
+    def mix(before, own, start, c):
+        place = start + lax.broadcasted_iota(jnp.int32, (own.shape[0], group_width), 0)
+        out = []
+        for g in range(groups_here):
+            lanes = slice(g * group_width, (g + 1) * group_width)
+            here = own[:, lanes]
+            total = jnp.concatenate([before[:, lanes], here], axis=0)
+            span = 1
+            while span < windows[g % 4]:
+                total = total + pltpu.roll(total, span, 0)
+                span = span * 2
+            divisor = jnp.minimum(place + 1, span).astype(f32)
+            contrast = (total[halo_rows:] / divisor - here).astype(bf16)
+            group = c * groups_here + g
+            mapped = jnp.dot(contrast, maps[group], preferred_element_type=f32)
+            out.append((mapped * scale[group]).astype(bf16))
+        return jnp.concatenate(out, axis=1)
+
+    for i in (0, 3, 4):
+        loads[i].wait()
+    for c in range(cores):
+        start = c * half
+        before = pool[max(start - halo_rows, 0) : max(start, halo_rows)].astype(f32)
+        if c == 0:
+            before = jnp.zeros_like(before)
+        mixed[c] = mix(before, pool[start : start + half].astype(f32), sp * rows + start, core)
+
+    pl.semaphore_wait(
+        pltpu.get_barrier_semaphore(),
+        layers - 1 + peers - 1 + jnp.where(gives_halo, 1, 0),
+    )
+
+    def halo_copy(source):
+        return remote(
+            pool.at[pl.ds(rows - halo_rows, halo_rows)], halo.at[source], h_send.at[0],
+            h_recv.at[0, source], (jnp.minimum(sp + 1, size_sp - 1), 0),
+        )
+
+    def head_copy(source):
+        return remote(
+            pool.at[pl.ds(0, halo_rows)], head.at[source], h_send.at[1],
+            h_recv.at[1, source], (sp, 0),
+        )
+
+    def swap_copy(p, source):
+        return remote(
+            mixed.at[p], swapped.at[source], x_send.at[p], x_recv.at[source], (sp, p)
+        )
+
+    @pl.when(gives_halo)
+    def _():
+        halo_copy(core).start()
+
+    for o in range(1, cores):
+        swap_copy((core + o) % cores, core).start()
+
+    gives_head = jnp.logical_and(sp > 0, core > 0)
+
+    @pl.when(gives_head)
+    def _():
+        head_copy(core).start()
+
+    def meta_copy(target, source):
+        return remote(
+            metas.at[source], metas.at[source], m_send.at[target], m_recv.at[source],
+            in_column(target),
+        )
+
+    for load in loads[8:11]:
+        load.start()
+
+    def neighbour(side):
+        return in_column(jnp.clip(jnp.where(side == 0, z + 1, z - 1), 0, layers - 1))
+
+    def chunk_copy(s, k, side):
+        return remote(
+            gathered.at[s, k], gathered.at[s, k], z_send.at[side, s], z_recv.at[s, k],
+            neighbour(side),
+        )
+
+    def pack_copy(s, k, p, source):
+        return remote(
+            packed.at[s, k, p], arrived.at[s, k, source], a_send.at[s],
+            a_recv.at[s], in_layer(p),
+        )
+
+    def back_copy(s, k, p, source):
+        return remote(
+            results.at[s, k, p], back.at[s, k, source], b_send.at[s],
+            b_recv.at[s, k], in_layer(p),
+        )
+
+    def own_pack(s, k):
+        return pltpu.make_async_copy(
+            packed.at[s, k, me], arrived.at[s, k, me], a_recv.at[s]
+        )
+
+    def own_back(s, k):
+        return pltpu.make_async_copy(
+            results.at[s, k, me], back.at[s, k, me], b_recv.at[s, k]
+        )
+
+    def part_copy(s, k, side):
+        slot = jnp.where(jnp.logical_and(side == 1, s == z - 1), layers, s)
+        return remote(
+            part.at[s, k], landed.at[slot, k], c_send.at[s], c_recv.at[slot, k],
+            neighbour(side),
+        )
+
+    def wait_bytes(ref, sem):
+        pltpu.make_async_copy(ref, ref, sem).wait()
+
+    far_first = sorted(range(1, peers), key=lambda o: (o % cores, -o % 3, o))
+
+    for load in loads[11:]:
+        load.start()
     loads[1].wait()
     loads[2].wait()
     experts = layers * peers
@@ -246,126 +404,9 @@
     ]
     metas[z] = jnp.concatenate(slot + [shares], axis=0)
 
-    half = rows // cores
-
-    def mix(before, own, start, c):
-        place = start + lax.broadcasted_iota(jnp.int32, (own.shape[0], group_width), 0)
-        out = []
-        for g in range(groups_here):
-            lanes = slice(g * group_width, (g + 1) * group_width)
-            here = own[:, lanes]
-            total = jnp.concatenate([before[:, lanes], here], axis=0)
-            span = 1
-            while span < windows[g % 4]:
-                total = total + pltpu.roll(total, span, 0)
-                span = span * 2
-            divisor = jnp.minimum(place + 1, span).astype(f32)
-            contrast = (total[halo_rows:] / divisor - here).astype(bf16)
-            group = c * groups_here + g
-            mapped = jnp.dot(contrast, maps[group], preferred_element_type=f32)
-            out.append((mapped * scale[group]).astype(bf16))
-        return jnp.concatenate(out, axis=1)
-
-    for i in (0, 3, 4):
-        loads[i].wait()
-    for c in range(cores):
-        start = c * half
-        before = pool[max(start - halo_rows, 0) : max(start, halo_rows)].astype(f32)
-        if c == 0:
-            before = jnp.zeros_like(before)
-        mixed[c] = mix(before, pool[start : start + half].astype(f32), sp * rows + start, core)
-
-    pl.semaphore_wait(
-        pltpu.get_barrier_semaphore(),
-        layers - 1 + peers - 1 + jnp.where(gives_halo, 1, 0),
-    )
-
-    def halo_copy(source):
-        return remote(
-            pool.at[pl.ds(rows - halo_rows, halo_rows)], halo.at[source], h_send.at[0],
-            h_recv.at[0, source], (jnp.minimum(sp + 1, size_sp - 1), 0),
-        )
-
-    def head_copy(source):
-        return remote(
-            pool.at[pl.ds(0, halo_rows)], head.at[source], h_send.at[1],
-            h_recv.at[1, source], (sp, 0),
-        )
-
-    def swap_copy(p, source):
-        return remote(
-            mixed.at[p], swapped.at[source], x_send.at[p], x_recv.at[source], (sp, p)
-        )
-
-    @pl.when(gives_halo)
-    def _():
-        halo_copy(core).start()
-
-    for o in range(1, cores):
-        swap_copy((core + o) % cores, core).start()
-
-    gives_head = jnp.logical_and(sp > 0, core > 0)
-
-    @pl.when(gives_head)
-    def _():
-        head_copy(core).start()
-
-    def meta_copy(target, source):
-        return remote(
-            metas.at[source], metas.at[source], m_send.at[target], m_recv.at[source],
-            in_column(target),
-        )
-
     for o in range(1, layers):
         meta_copy((z + o) % layers, z).start()
-    for load in loads[8:11]:
-        load.start()
-
-    def neighbour(side):
-        return in_column(jnp.clip(jnp.where(side == 0, z + 1, z - 1), 0, layers - 1))
-
-    def chunk_copy(s, k, side):
-        return remote(
-            gathered.at[s, k], gathered.at[s, k], z_send.at[side, s], z_recv.at[s, k],
-            neighbour(side),
-        )
-
-    def pack_copy(s, k, p, source):
-        return remote(
-            packed.at[s, k, p], arrived.at[s, k, source], a_send.at[s],
-            a_recv.at[s], in_layer(p),
-        )
-
-    def back_copy(s, k, p, source):
-        return remote(
-            results.at[s, k, p], back.at[s, k, source], b_send.at[s],
-            b_recv.at[s, k], in_layer(p),
-        )
-
-    def own_pack(s, k):
-        return pltpu.make_async_copy(
-            packed.at[s, k, me], arrived.at[s, k, me], a_recv.at[s]
-        )
-
-    def own_back(s, k):
-        return pltpu.make_async_copy(
-            results.at[s, k, me], back.at[s, k, me], b_recv.at[s, k]
-        )
-
-    def part_copy(s, k, side):
-        slot = jnp.where(jnp.logical_and(side == 1, s == z - 1), layers, s)
-        return remote(
-            part.at[s, k], landed.at[slot, k], c_send.at[s], c_recv.at[slot, k],
-            neighbour(side),
-        )
-
-    def wait_bytes(ref, sem):
-        pltpu.make_async_copy(ref, ref, sem).wait()
-
-    far_first = sorted(range(1, peers), key=lambda o: (o % cores, -o % 3, o))
-
-    for load in loads[11:]:
-        load.start()
+
     for o in range(1, cores):
         p = (core + o) % cores
         swap_copy(p, p).wait_recv()
@@ -480,12 +521,12 @@
         tall = jnp.concatenate(
             [arrived[s, k].reshape(slots, cols) for k in range(blocks)], axis=1
         )
-        hidden = mlp(tall, eg, eu)
-        for k in range(blocks):
-            got = jnp.dot(hidden, ed[:, k * cols : (k + 1) * cols], preferred_element_type=f32)
-            results[s, k] = got.astype(bf16).reshape(peers, cap, cols)
+        hidden[s] = mlp(tall, eg, eu)
 
     def give_back(s, k):
+        lanes = pl.ds(pl.multiple_of(k * cols, cols), cols)
+        got = jnp.dot(hidden[s], ed[:, lanes], preferred_element_type=f32)
+        results[s, k] = got.astype(bf16).reshape(peers, cap, cols)
         for o in far_first:
             back_copy(s, k, (me + o) % peers, me).start()
         own_back(s, k).start()
@@ -526,28 +567,29 @@
         for load in loads[8:11]:
             load.wait()
         tall = jnp.concatenate([gathered[z, k] for k in range(blocks)], axis=1)
-        hidden = mlp(tall, sg, su)
+        inner = mlp(tall, sg, su)
         for k in range(blocks):
             acc[k] = acc[k] + jnp.dot(
-                hidden, sd[:, k * cols : (k + 1) * cols], preferred_element_type=f32
+                inner, sd[:, k * cols : (k + 1) * cols], preferred_element_type=f32
             )
 
-    plans = [
-        [code_of(step, layers, blocks) for step in steps_of(s, layers, blocks)]
+    plans = {
+        (s, c): [code_of(step, layers, blocks) for step in steps_of(s, c, layers, blocks)]
         for s in range(layers)
-    ]
+        for c in range(cores)
+    }
     nothing = 3 * area + layers + 1
     base = 1 << nothing.bit_length()
     per_word = 30 // nothing.bit_length()
-    count = -(-max(len(plan) for plan in plans) // per_word)
+    count = -(-max(len(plan) for plan in plans.values()) // per_word)
     words = []
     for i in range(count):
         word = jnp.int32(0)
-        for s, plan in enumerate(plans):
+        for (s, c), plan in plans.items():
             codes = plan[i * per_word : (i + 1) * per_word]
             codes = codes + [nothing] * (per_word - len(codes))
             packed_codes = sum(code * base**j for j, code in enumerate(codes))
-            word = jnp.where(z == s, packed_codes, word)
+            word = jnp.where(jnp.logical_and(z == s, core == c), packed_codes, word)
         words.append(word)
 
     def act(code):
@@ -692,6 +734,7 @@
             pltpu.VMEM(chunks, bf16),
             pltpu.VMEM((layers + 1, blocks, tokens, cols), bf16),
             pltpu.VMEM((blocks, tokens, cols), f32),
+            pltpu.VMEM((layers, slots, expert_width), bf16),
             pltpu.VMEM((width, hidden_width), bf16),
             pltpu.VMEM((width, hidden_width), bf16),
             pltpu.VMEM((hidden_width, width), bf16),

time: 83 us -> 82.1 us (0.989)
  Pallas kernels: 82 us -> 81.1 us
    pallas_call x1, Pallas kernels: 82 us -> 81.1 us  [on_device(): pl.pallas_call(functools.partial(layer_kernel, layers, peers, cores, cap)...]
where the time goes in v5:
time: 82.1 us; the launch traced here: 81.9 us
  Pallas kernels  81.1 us (99%)
    pallas_call x1, Pallas kernels, on_device(): pl.pallas_call(functools.partial(layer_kernel, layers, peers, cores, cap)...  81.1 us

profile of v5, /device:TPU:0, one launch (start us, length us, event | category | flops | bytes accessed | tf_op | source)
XLA Modules:
  0.0 81.9 jit_solution(10274067945012415770)
XLA Ops:
  0.0 81.1 %shard_map.136 = bf16[128,2048]{1,0:T(8,128)(2,1)S(1)} custom-call(bf16[128,2048]{1,0:T(8,128)(2,1)} %residual_hbm.1, bf16[256,512]{1,0:T(8,128)(2,1)} %pool_hbm.1, bf16[8,128,128]{2,1,0:T(8,128)(2,1)} %maps_hbm.1, f32[8,1,128]{2,1,0:T(1,128)} %bitcast.5, bf16[1024,2048]{1,0:T(8,128)(2,1)} %proj_hbm.1, f32[1,2048]{1,0:T(1,128)} %bitcast.4, ...), custom_call_target="tpu_custom_call" | custom-call | tf_op jit(solution)/shard_map/pallas_call | solution.py:708
  81.1 0.8 copy.16

commit v6 on v5

--- a/solution.py
+++ b/solution.py
@@ -407,6 +407,23 @@
     for o in range(1, layers):
         meta_copy((z + o) % layers, z).start()
 
+    for load in loads[5:8]:
+        load.wait()
+
+    def channels_of(c):
+        return pl.ds(pl.multiple_of(c * channels, channels), channels)
+
+    def project_own():
+        for k in range(blocks):
+            lanes = slice(k * cols, (k + 1) * cols)
+            acc[k] = residual[:, lanes].astype(f32) + jnp.dot(
+                mixed[core], proj[channels_of(core), lanes], preferred_element_type=f32
+            )
+
+    @pl.when(jnp.logical_not(takes_halo))
+    def _():
+        project_own()
+
     for o in range(1, cores):
         p = (core + o) % cores
         swap_copy(p, p).wait_recv()
@@ -425,17 +442,13 @@
             else:
                 swapped[c, :halo_rows] = fixed
 
-    for load in loads[5:8]:
-        load.wait()
-
-    def channels_of(c):
-        return pl.ds(pl.multiple_of(c * channels, channels), channels)
+    @pl.when(takes_halo)
+    def _():
+        project_own()
 
     for k in range(blocks):
         lanes = slice(k * cols, (k + 1) * cols)
-        total = residual[:, lanes].astype(f32) + jnp.dot(
-            mixed[core], proj[channels_of(core), lanes], preferred_element_type=f32
-        )
+        total = acc[k]
         for o in range(1, cores):
             p = (core + o) % cores
             total = total + jnp.dot(

time: 82.1 us -> 81.7 us (level)
  no operation moved by 1% of the time
where the time goes in v6:
time: 81.7 us; the launch traced here: 81.5 us
  Pallas kernels  80.7 us (99%)
    pallas_call x1, Pallas kernels, on_device(): pl.pallas_call(functools.partial(layer_kernel, layers, peers, cores, cap)...  80.7 us

profile of v6, /device:TPU:0, one launch (start us, length us, event | category | flops | bytes accessed | tf_op | source)
XLA Modules:
  0.0 81.5 jit_solution(1607768092772444885)
XLA Ops:
  0.0 80.7 %shard_map.136 = bf16[128,2048]{1,0:T(8,128)(2,1)S(1)} custom-call(bf16[128,2048]{1,0:T(8,128)(2,1)} %residual_hbm.1, bf16[256,512]{1,0:T(8,128)(2,1)} %pool_hbm.1, bf16[8,128,128]{2,1,0:T(8,128)(2,1)} %maps_hbm.1, f32[8,1,128]{2,1,0:T(1,128)} %bitcast.5, bf16[1024,2048]{1,0:T(8,128)(2,1)} %proj_hbm.1, f32[1,2048]{1,0:T(1,128)} %bitcast.4, ...), custom_call_target="tpu_custom_call" | custom-call | tf_op jit(solution)/shard_map/pallas_call | solution.py:721
  80.7 0.8 copy.16
